TPU v7x, 32 devices: a whole 2x2x4 slice. The times are simulated.
32 devices in a mesh: sp: 4 (over z), tp: 4 (over y, x), dp: 2 (over core).
Axes of the slice: x: 2, y: 2, z: 4, core: 2. Of those that a mesh axis runs over, the one named last changes fastest.
Arguments:
- latents: bfloat16 [1024, 2048], P(('dp', 'sp', 'tp')), parts along dimension 0, may hold values from -6 to 6
- sample_vector: float32 [2, 2048], P('dp'), parts along dimension 0, may hold values from -6 to 6
- context: bfloat16 [512, 2048], P(('dp', 'sp')), parts along dimension 0, may hold values from -6 to 6
- context_vector: float32 [1, 2048], replicated, may hold values from -6 to 6
- norm_gain: float32 [2048], replicated, may hold values from 0.1 to 1.9
- modulator: bfloat16 [2048, 6144], P(None, ('sp', 'tp')), may hold values from -0.25 to 0.25
- query_weight: bfloat16 [2048, 1024], P('sp', 'tp'), may hold values from -0.125 to 0.125
- key_weight: bfloat16 [2048, 1024], P('sp', 'tp'), may hold values from -0.125 to 0.125
- value_weight: bfloat16 [2048, 2048], P('sp', 'tp'), may hold values from -0.125 to 0.125
- decay_down: bfloat16 [2048, 64], replicated, may hold values from -0.125 to 0.125
- decay_up: bfloat16 [2, 32, 1024], P(None, None, 'tp'), may hold values from -1 to 1
- decay_bias: float32 [2, 1024], P(None, 'tp'), as said below
- decay_extra: float32 [2, 1024, 8], P(None, ('dp', 'sp'), 'tp'), parts along dimension 1, may hold values from -2 to 0
- head_gain: float32 [256], replicated, may hold values from 0.1 to 1.9
- out_weight: bfloat16 [2048, 2048], P('tp'), may hold values from -0.125 to 0.125
Outputs:
- updated: bfloat16 [1024, 2048], P(('dp', 'sp', 'tp')), parts along dimension 0
There are 2 independent parts, one for each index of `dp`. A program takes and returns all parts, laid end to end along the dimension named above; an argument that names none is the same for every part. Nothing has to cross between parts.
Inputs may be any that keep to these rules, and one draw needn't show every extreme that they name: `decay_bias`: offsets of the decay gates,.
All inputs are finite; a program needn't handle non-finite values.
Results may differ from a plain program's by a relative error of at most 0.012.
Values may be sent and summed in bfloat16 or wider, within the bound.
A program may use at most 64 MiB of HBM per device.

v0:
```python
import functools

import jax
import jax.numpy as jnp
from jax import lax
from jax.experimental import pallas as pl
from jax.experimental.pallas import tpu as pltpu
from jax.sharding import PartitionSpec as P

DK = 128
BLOCK = 64
CTX_LIFT = 4
EPS = 1e-06
SHARP = 16.0
F32 = jnp.float32
BF16 = jnp.bfloat16
MESH = pl.DeviceIdType.MESH
HIGH = lax.Precision.HIGHEST


def dot(a, b):
    return jnp.dot(a, b, preferred_element_type=F32)


def dot_nt(a, b):
    return lax.dot_general(a, b, (((1,), (1,)), ((), ())), preferred_element_type=F32)


def dot_tn(a, b):
    return lax.dot_general(a, b, (((0,), (0,)), ((), ())), preferred_element_type=F32)


def sums(mask, values):
    return jnp.dot(mask.astype(F32), values, precision=HIGH, preferred_element_type=F32)


def log_sigmoid(x):
    return jnp.minimum(x, 0.0) - jnp.log1p(jnp.exp(-jnp.abs(x)))


def kernel(
    n_sp,
    n_tp,
    latents_in,
    sample_vector_in,
    context_in,
    context_vector_in,
    norm_gain_in,
    modulator,
    query_weight,
    key_weight,
    value_weight,
    decay_down_in,
    decay_up_in,
    decay_bias_in,
    decay_extra_in,
    head_gain_in,
    out_weight,
    out,
    latents,
    sample_vector,
    context,
    context_vector,
    norm_gain,
    decay_down,
    decay_up,
    decay_bias,
    decay_extra,
    head_gain,
    mod_w,
    mods,
    lat,
    hid,
    wk,
    wv,
    wq,
    wo,
    acc_k,
    acc_v,
    acc_q,
    cbuf,
    st_own,
    st_in,
    st_out,
    normed,
    part,
    rs,
    loc_sem,
    mod_s,
    mod_r,
    lat_s,
    lat_r,
    w_s,
    w_r,
    p_s,
    p_r,
    cz_s,
    cz_r,
    ct_s,
    ct_r,
    st_s,
    st_r,
    rs_s,
    rs_r,
):
    s = lax.axis_index("sp")
    t = lax.axis_index("tp")
    d = lax.axis_index("dp")
    h = lax.rem(d, 2)
    mate = d + 1 - 2 * h
    n_dev = n_sp * n_tp
    me = s * n_tp + t
    rows, width = latents.shape
    ctx_rows = context.shape[0]
    length = rows * n_tp
    total = hid.shape[1]
    ctx_all = n_sp * ctx_rows
    depth = hid.shape[2]
    half = depth // 2
    heads = decay_bias.shape[1] // DK
    dv = head_gain.shape[1]
    rank = decay_up.shape[1]

    def peer(k):
        other = lax.rem(me + k, n_dev)
        return {"sp": other // n_tp, "tp": lax.rem(other, n_tp)}

    weights = ((key_weight, wk), (value_weight, wv), (query_weight, wq))
    local = [pltpu.make_async_copy(modulator, mod_w, loc_sem.at[0])]
    for m, (source, slots) in enumerate(weights):
        for i in range(2):
            local.append(
                pltpu.make_async_copy(
                    source.at[pl.ds(i * half, half)], slots.at[s, i], loc_sem.at[1 + 2 * m + i]
                )
            )
    local.append(pltpu.make_async_copy(out_weight, wo, loc_sem.at[7]))
    barrier = pltpu.get_barrier_semaphore()
    for k in range(1, n_dev):
        pl.semaphore_signal(barrier, inc=1, device_id=peer(k), device_id_type=MESH)
    pl.semaphore_signal(barrier, inc=1, device_id={"dp": mate}, device_id_type=MESH)
    small = [
        pltpu.make_async_copy(source, target, loc_sem.at[8 + i])
        for i, (source, target) in enumerate(
            (
                (sample_vector_in, sample_vector),
                (context_vector_in, context_vector),
                (latents_in, latents),
                (context_in, context),
                (norm_gain_in, norm_gain),
                (decay_down_in, decay_down),
                (decay_up_in, decay_up),
                (decay_bias_in, decay_bias),
                (decay_extra_in, decay_extra),
                (head_gain_in, head_gain),
            )
        )
    ]
    for copy in small[:4] + local[:1] + small[4:] + local[1:]:
        copy.start()
    small[2].wait()
    small[3].wait()
    pl.semaphore_wait(barrier, n_dev)

    def ring_copy(m, r, j, first=False):
        source, slots = weights[m]
        origin = s - j if r == 0 else s + j
        target = s + 1 if r == 0 else s - 1
        src = source.at[pl.ds(h * half, half)] if first else slots.at[origin, h]
        return pltpu.make_async_remote_copy(
            src_ref=src,
            dst_ref=slots.at[origin, h],
            send_sem=w_s.at[m, r, j],
            recv_sem=w_r.at[m, r, j],
            device_id={"sp": target},
            device_id_type=MESH,
        )

    def ring_arrival(m, r, j):
        slots = weights[m][1]
        origin = s - j if r == 0 else s + j
        return pltpu.make_async_remote_copy(
            src_ref=slots.at[origin, h],
            dst_ref=slots.at[origin, h],
            send_sem=w_s.at[m, r, j - 1],
            recv_sem=w_r.at[m, r, j - 1],
            device_id={"sp": s},
            device_id_type=MESH,
        )

    def mate_copy(m, r, j, side):
        slots = weights[m][1]
        origin = s - j if r == 0 else s + j
        return pltpu.make_async_remote_copy(
            src_ref=slots.at[origin, side],
            dst_ref=slots.at[origin, side],
            send_sem=p_s.at[m, r, j - 1],
            recv_sem=p_r.at[m, r, j - 1],
            device_id={"dp": mate},
            device_id_type=MESH,
        )

    def exists(r, j):
        return s - j >= 0 if r == 0 else s + j < n_sp

    def onward(r):
        return s + 1 < n_sp if r == 0 else s - 1 >= 0

    def send_own(m):
        for r in range(2):

            @pl.when(onward(r))
            def _():
                ring_copy(m, r, 0, True).start()

    def relay(m, j):
        for r in range(2):

            @pl.when(exists(r, j))
            def _():
                ring_arrival(m, r, j).wait_recv()
                if j < n_sp - 1:

                    @pl.when(onward(r))
                    def _():
                        ring_copy(m, r, j).start()

                mate_copy(m, r, j, h).start()

    def whole(slots, o):
        return slots[o].reshape(depth, slots.shape[3])

    def multiply(m, j, acc, count):
        slots = weights[m][1]
        for r in range(2):

            @pl.when(exists(r, j))
            def _():
                origin = s - j if r == 0 else s + j
                mate_copy(m, r, j, 1 - h).wait_recv()
                acc[...] += dot(hid[origin, 0:count], whole(slots, origin))

    lat_copies = []
    for k in range(1, n_tp):
        lat_copies.append(
            pltpu.make_async_remote_copy(
                src_ref=latents,
                dst_ref=lat.at[t],
                send_sem=lat_s.at[k],
                recv_sem=lat_r.at[k],
                device_id={"tp": lax.rem(t + k, n_tp)},
                device_id_type=MESH,
            )
        )
    span_t = width // n_tp

    def ctx_line(k):
        return pltpu.make_async_remote_copy(
            src_ref=context.at[:, pl.ds(t * span_t, span_t)],
            dst_ref=cbuf.at[s, :, pl.ds(t * span_t, span_t)],
            send_sem=cz_s.at[k],
            recv_sem=cz_r.at[k],
            device_id={"sp": lax.rem(s + k, n_sp)},
            device_id_type=MESH,
        )

    def ctx_line_arrival(k):
        return pltpu.make_async_remote_copy(
            src_ref=context.at[:, pl.ds(t * span_t, span_t)],
            dst_ref=cbuf.at[lax.rem(s - k + n_sp, n_sp), :, pl.ds(t * span_t, span_t)],
            send_sem=cz_s.at[k],
            recv_sem=cz_r.at[k],
            device_id={"sp": s},
            device_id_type=MESH,
        )

    def ctx_plane(k, u, owner):
        view = cbuf.at[lax.rem(s - k + n_sp, n_sp), :, pl.ds(owner * span_t, span_t)]
        return pltpu.make_async_remote_copy(
            src_ref=view,
            dst_ref=view,
            send_sem=ct_s.at[k, u],
            recv_sem=ct_r.at[k, u],
            device_id={"tp": lax.rem(t + u, n_tp)},
            device_id_type=MESH,
        )

    for k in range(1, n_sp):
        ctx_line(k).start()
    for copy in lat_copies:
        copy.start()
    send_own(0)
    send_own(1)
    queue = [(m, j) for j in range(1, n_sp) for m in range(2)]

    def relay_next():
        if queue:
            m, j = queue.pop(0)
            relay(m, j)
            if (m, j) == (1, max(n_sp - 2, 1)):
                send_own(2)

    small[0].wait()
    small[1].wait()
    is_first = lax.broadcasted_iota(jnp.int32, (16, width), 0) == 0
    vectors = jnp.where(is_first, sample_vector[...], context_vector[...])
    conditions = (vectors / (1.0 + jnp.exp(-vectors))).astype(BF16)
    local[0].wait()
    mods[me] = dot(conditions, mod_w[...])[0:2]
    mod_copies = []
    for k in range(1, n_dev):
        copy = pltpu.make_async_remote_copy(
            src_ref=mods.at[me],
            dst_ref=mods.at[me],
            send_sem=mod_s.at[k],
            recv_sem=mod_r.at[k],
            device_id=peer(k),
            device_id_type=MESH,
        )
        copy.start()
        mod_copies.append(copy)

    for k in range(1, n_sp):
        ctx_line_arrival(k).wait_recv()
        for u in range(1, n_tp):
            ctx_plane(k, u, t).start()
    relay_next()
    lat[t] = latents[...]
    cbuf[s] = context[...]
    for k in range(1, n_tp):
        pltpu.make_async_remote_copy(
            src_ref=latents,
            dst_ref=lat.at[lax.rem(t - k + n_tp, n_tp)],
            send_sem=lat_s.at[k],
            recv_sem=lat_r.at[k],
            device_id={"tp": t},
            device_id_type=MESH,
        ).wait_recv()
    for k in range(1, n_dev):
        other = lax.rem(me - k + n_dev, n_dev)
        pltpu.make_async_remote_copy(
            src_ref=mods.at[me],
            dst_ref=mods.at[other],
            send_sem=mod_s.at[k],
            recv_sem=mod_r.at[k],
            device_id={"tp": t},
            device_id_type=MESH,
        ).wait_recv()
    for copy in small[4:]:
        copy.wait()
    modulation = jnp.concatenate([mods[i] for i in range(n_dev)], axis=1)
    gate = modulation[0:1, 2 * width :]

    def modulated(x, row):
        x = x.astype(F32)
        x = x * lax.rsqrt(jnp.mean(x * x, axis=-1, keepdims=True) + EPS) * norm_gain[...]
        shift = modulation[row : row + 1, :width]
        scale = modulation[row : row + 1, width : 2 * width]
        return (x * (1.0 + scale) + shift).astype(BF16)

    def put(x, at):
        count = x.shape[0]
        for o in range(n_sp):
            hid[o, at : at + count] = x[:, o * depth : (o + 1) * depth]

    for i in range(n_tp):
        put(modulated(lat[i], 0), i * rows)
    relay_next()
    for k in range(1, n_sp):
        for u in range(1, n_tp):
            ctx_plane(k, u, lax.rem(t - u + n_tp, n_tp)).wait_recv()
    piece = min(32, ctx_rows)
    for o in range(n_sp):
        for i in range(ctx_rows // piece):
            put(
                modulated(cbuf[o, i * piece : (i + 1) * piece], 1),
                length + o * ctx_rows + i * piece,
            )

    low = dot_nt(hid[0], decay_down[:, 0:depth])
    for o in range(1, n_sp):
        low = low + dot_nt(hid[o], decay_down[:, o * depth : (o + 1) * depth])
    low = low.astype(BF16)

    relay_next()

    def log_decays(values, z):
        x = dot(values[:, z * rank : (z + 1) * rank], decay_up[z]) + decay_bias[z : z + 1]
        return log_sigmoid(x) / SHARP

    row_id = lax.broadcasted_iota(jnp.int32, (length, length), 0)
    col_id = lax.broadcasted_iota(jnp.int32, (length, length), 1)
    same = row_id // BLOCK == col_id // BLOCK
    inner = [same & (col_id <= row_id), same & (col_id >= row_id)]

    def extra_sums(z):
        columns = [
            jnp.sum(jnp.where(inner[z], decay_extra[z, g : g + 1, :], 0.0), axis=1, keepdims=True)
            for g in range(heads)
        ]
        return jnp.concatenate([jnp.broadcast_to(c, (length, DK)) for c in columns], axis=1)

    within = [sums(inner[z], log_decays(low[:length], z)) + extra_sums(z) for z in range(2)]
    blocks = length // BLOCK
    totals = [
        [within[0][(b + 1) * BLOCK - 1 : (b + 1) * BLOCK] for b in range(blocks)],
        [within[1][b * BLOCK : b * BLOCK + 1] for b in range(blocks)],
    ]
    none = jnp.zeros_like(totals[0][0])

    def between(z, lo, hi):
        value = none
        for b in range(lo, hi):
            value = value + totals[z][b]
        return value

    lows = low[length:]
    crow = lax.broadcasted_iota(jnp.int32, (ctx_all, ctx_all), 0)
    ccol = lax.broadcasted_iota(jnp.int32, (ctx_all, ctx_all), 1)
    ctx_weight = [
        jnp.exp(sums(ccol > crow, log_decays(lows, 0))),
        jnp.exp(sums(ccol < crow, log_decays(lows, 1))),
    ]

    for copy in local[1:5]:
        copy.wait()
    acc_k[...] = dot(hid[s], whole(wk, s))
    acc_v[...] = dot(hid[s], whole(wv, s))
    multiply(0, 1, acc_k, total)
    relay_next()
    multiply(1, 1, acc_v, total)
    for j in range(2, n_sp):
        relay_next()
        multiply(0, j, acc_k, total)
        relay_next()
        multiply(1, j, acc_v, total)
    keys = acc_k[...].astype(BF16)
    values = acc_v[...].astype(BF16)
    ckeys = keys[length:].astype(F32)
    cvals = values[length:]
    keys = keys[:length].astype(F32)
    values = values[:length]

    def per_block(f):
        return jnp.concatenate([f(b) for b in range(blocks)], axis=0)

    def rows_of(x, b):
        return x[b * BLOCK : (b + 1) * BLOCK]

    ending = [
        jnp.exp(
            per_block(
                lambda b: totals[0][b] - rows_of(within[0], b) + between(0, b + 1, blocks)
            )
        ),
        jnp.exp(per_block(lambda b: totals[1][b] - rows_of(within[1], b) + between(1, 0, b))),
    ]
    for z in range(2):
        ended = (keys * ending[z]).astype(BF16)
        for g in range(heads):
            st_own[z, g] = dot_tn(
                values[:, g * dv : (g + 1) * dv], ended[:, g * DK : (g + 1) * DK]
            )

    def begins(z):
        return s == 0 if z == 0 else s == n_sp - 1

    def goes_on(z):
        return s < n_sp - 1 if z == 0 else s > 0

    def state_copy(z, g):
        return pltpu.make_async_remote_copy(
            src_ref=st_out.at[z, g],
            dst_ref=st_in.at[z, g],
            send_sem=st_s.at[z, g],
            recv_sem=st_r.at[z, g],
            device_id={"sp": s + 1 if z == 0 else s - 1},
            device_id_type=MESH,
        )

    whole_decay = [jnp.exp(between(z, 0, blocks)) for z in range(2)]

    def pass_on(z, g):
        @pl.when(goes_on(z))
        def _():
            decay = whole_decay[z][:, g * DK : (g + 1) * DK]
            st_out[z, g] = (st_in[z, g].astype(F32) * decay + st_own[z, g]).astype(BF16)
            state_copy(z, g).start()

    for z in range(2):

        @pl.when(begins(z))
        def _():
            ended = (ckeys * ctx_weight[z]).astype(BF16)
            for g in range(heads):
                st_in[z, g] = (
                    CTX_LIFT
                    * dot_tn(cvals[:, g * dv : (g + 1) * dv], ended[:, g * DK : (g + 1) * DK])
                ).astype(BF16)
                pass_on(z, g)

    def chain(near):
        for z in range(2):
            ahead = 2 * s < n_sp - 1 if z == 0 else 2 * s >= n_sp - 1
            turn = ahead if near else jnp.logical_not(ahead)

            @pl.when(jnp.logical_and(turn, jnp.logical_not(begins(z))))
            def _():
                for g in range(heads):
                    state_copy(z, g).wait_recv()
                    pass_on(z, g)

    for copy in local[5:7]:
        copy.wait()
    acc_q[...] = dot(hid[s, 0:length], whole(wq, s))
    for j in range(1, n_sp):
        relay(2, j)
        if j == 1:
            chain(True)
        multiply(2, j, acc_q, length)
        if j == max(n_sp - 2, 1):
            chain(False)
    queries = acc_q[...].astype(BF16).astype(F32)

    tri_row = lax.broadcasted_iota(jnp.int32, (BLOCK, BLOCK), 0)
    tri_col = lax.broadcasted_iota(jnp.int32, (BLOCK, BLOCK), 1)
    masks = [tri_col <= tri_row, tri_col >= tri_row]
    query_dec = [(queries * jnp.exp(within[z])).astype(BF16) for z in range(2)]
    key_dec = [(keys * jnp.exp(-within[z])).astype(BF16) for z in range(2)]
    near = [
        keys * jnp.exp(per_block(lambda b: totals[z][b] - rows_of(within[z], b)))
        for z in range(2)
    ]
    lifted = [
        (queries * jnp.exp(within[0] + per_block(lambda b: between(0, 0, b) + jnp.zeros((BLOCK, 1), F32)))).astype(BF16),
        (queries * jnp.exp(within[1] + per_block(lambda b: between(1, b + 1, blocks) + jnp.zeros((BLOCK, 1), F32)))).astype(BF16),
    ]
    local_out = []
    for g in range(heads):
        cs = slice(g * DK, (g + 1) * DK)
        score_rows = []
        for i in range(blocks):
            line = []
            for j in range(blocks):
                if i == j:
                    score = 0.0
                    for z in range(2):
                        inner = dot_nt(
                            rows_of(query_dec[z], i)[:, cs], rows_of(key_dec[z], j)[:, cs]
                        )
                        score = score + jnp.where(masks[z], inner, 0.0)
                else:
                    z = 0 if j < i else 1
                    gap = between(z, min(i, j) + 1, max(i, j))
                    far = (rows_of(near[z], j) * jnp.exp(gap)).astype(BF16)
                    score = dot_nt(rows_of(query_dec[z], i)[:, cs], far[:, cs])
                line.append(score)
            score_rows.append(jnp.concatenate(line, axis=1))
        scores = jnp.concatenate(score_rows, axis=0).astype(BF16)
        local_out.append(dot(scores, values[:, g * dv : (g + 1) * dv]))

    for g in range(heads):
        mixed = local_out[g]
        for z in range(2):
            mixed = mixed + dot_nt(
                lifted[z][:, g * DK : (g + 1) * DK], st_in[z, g]
            )
        scale = lax.rsqrt(jnp.mean(mixed * mixed, axis=-1, keepdims=True) + EPS)
        normed[:, g * dv : (g + 1) * dv] = (mixed * scale * head_gain[...]).astype(BF16)

    local[7].wait()
    chunks = rs_s.shape[1]
    span = width // chunks
    rs_copies = []
    for c in range(chunks):
        cols = slice(c * span, (c + 1) * span)
        product = dot(normed[...], wo[:, cols]).astype(BF16)
        for i in range(n_tp):
            part[i, :, cols] = product[i * rows : (i + 1) * rows]
        for k in range(1, n_tp):
            to = lax.rem(t + k, n_tp)
            copy = pltpu.make_async_remote_copy(
                src_ref=part.at[to, :, pl.ds(c * span, span)],
                dst_ref=rs.at[k, :, pl.ds(c * span, span)],
                send_sem=rs_s.at[k, c],
                recv_sem=rs_r.at[k, c],
                device_id={"tp": to},
                device_id_type=MESH,
            )
            copy.start()
            rs_copies.append(copy)
    for c in range(chunks):
        cols = slice(c * span, (c + 1) * span)
        summed = part[t, :, cols].astype(F32)
        for k in range(1, n_tp):
            rs_copies[c * (n_tp - 1) + k - 1].wait_recv()
            summed = summed + rs[k, :, cols].astype(F32)
        projected = summed.astype(BF16).astype(F32)
        out[:, cols] = (latents[:, cols].astype(F32) + gate[:, cols] * projected).astype(BF16)

    for copy in rs_copies + lat_copies + mod_copies:
        copy.wait_send()
    for k in range(1, n_sp):
        ctx_line(k).wait_send()
        for u in range(1, n_tp):
            ctx_plane(k, u, t).wait_send()
    for z in range(2):

        @pl.when(goes_on(z))
        def _():
            for g in range(heads):
                state_copy(z, g).wait_send()

    for m in range(3):
        for r in range(2):

            @pl.when(onward(r))
            def _():
                ring_copy(m, r, 0, True).wait_send()

            for j in range(1, n_sp):

                @pl.when(exists(r, j))
                def _():
                    mate_copy(m, r, j, h).wait_send()
                    if j < n_sp - 1:

                        @pl.when(onward(r))
                        def _():
                            ring_copy(m, r, j).wait_send()


def per_device(n_sp, n_tp, *args):
    (latents, sv, context, cv, gain, modulator, wq, wk, wv, down, up, bias, extra, hg, wo) = args
    rows, width = latents.shape
    ctx_rows = context.shape[0]
    n_dev = n_sp * n_tp
    length = rows * n_tp
    total = length + n_sp * ctx_rows
    depth = wq.shape[0]
    kw, vw = wk.shape[1], wv.shape[1]
    heads = bias.shape[1] // DK
    dv = hg.shape[0]
    chunks = 4
    vmem = pl.BlockSpec(memory_space=pltpu.VMEM)
    hbm = pl.BlockSpec(memory_space=pl.ANY)
    dma = pltpu.SemaphoreType.DMA
    scratch = [
        pltpu.VMEM(latents.shape, BF16),
        pltpu.VMEM(sv.shape, F32),
        pltpu.VMEM(context.shape, BF16),
        pltpu.VMEM(cv.shape, F32),
        pltpu.VMEM((1, width), F32),
        pltpu.VMEM(down.shape[::-1], BF16),
        pltpu.VMEM(up.shape, BF16),
        pltpu.VMEM(bias.shape, F32),
        pltpu.VMEM((2, heads, length), F32),
        pltpu.VMEM((1, dv), F32),
        pltpu.VMEM(modulator.shape, BF16),
        pltpu.VMEM((n_dev, 2, modulator.shape[1]), F32),
        pltpu.VMEM((n_tp, rows, width), BF16),
        pltpu.VMEM((n_sp, total, depth), BF16),
        pltpu.VMEM((n_sp, 2, depth // 2, kw), BF16),
        pltpu.VMEM((n_sp, 2, depth // 2, vw), BF16),
        pltpu.VMEM((n_sp, 2, depth // 2, kw), BF16),
        pltpu.VMEM(wo.shape, BF16),
        pltpu.VMEM((total, kw), F32),
        pltpu.VMEM((total, vw), F32),
        pltpu.VMEM((length, kw), F32),
        pltpu.VMEM((n_sp, ctx_rows, width), BF16),
        pltpu.VMEM((2, heads, dv, DK), F32),
        pltpu.VMEM((2, heads, dv, DK), BF16),
        pltpu.VMEM((2, heads, dv, DK), BF16),
        pltpu.VMEM((length, vw), BF16),
        pltpu.VMEM((n_tp, rows, width), BF16),
        pltpu.VMEM((n_tp, rows, width), BF16),
        dma((18,)),
        dma((n_dev,)),
        dma((n_dev,)),
        dma((n_tp,)),
        dma((n_tp,)),
        dma((3, 2, n_sp)),
        dma((3, 2, n_sp)),
        dma((3, 2, n_sp)),
        dma((3, 2, n_sp)),
        dma((n_sp,)),
        dma((n_sp,)),
        dma((n_sp, n_tp)),
        dma((n_sp, n_tp)),
        dma((2, heads)),
        dma((2, heads)),
        dma((n_tp, chunks)),
        dma((n_tp, chunks)),
    ]
    return pl.pallas_call(
        functools.partial(kernel, n_sp, n_tp),
        out_shape=jax.ShapeDtypeStruct(latents.shape, BF16),
        in_specs=[hbm] * 15,
        out_specs=vmem,
        scratch_shapes=scratch,
        compiler_params=pltpu.CompilerParams(
            collective_id=0, has_side_effects=True, vmem_limit_bytes=56 * 1024 * 1024
        ),
    )(
        latents,
        sv,
        context,
        cv,
        gain.reshape(1, -1),
        modulator,
        wq,
        wk,
        wv,
        down.T,
        up,
        bias,
        extra.transpose(0, 2, 1),
        hg.reshape(1, -1),
        wo,
    )


def solution(mesh):
    placed = (
        P(("dp", "sp", "tp"), None),
        P("dp", None),
        P(("dp", "sp"), None),
        P(),
        P(),
        P(None, ("sp", "tp")),
        P("sp", "tp"),
        P("sp", "tp"),
        P("sp", "tp"),
        P(),
        P(None, None, "tp"),
        P(None, "tp"),
        P(None, ("dp", "sp"), "tp"),
        P(),
        P("tp", None),
    )
    return jax.shard_map(
        functools.partial(per_device, mesh.shape["sp"], mesh.shape["tp"]),
        mesh=mesh,
        in_specs=placed,
        out_specs=P(("dp", "sp", "tp"), None),
        check_vma=False,
    )
```

profile of v0, /device:TPU:0, one launch (start us, length us, event | category | flops | bytes accessed | tf_op | source)
XLA Modules:
  0.0 68.8 jit_solution(7599263260432708348)
XLA Ops:
  0.0 67.2 %shard_map.145 = bf16[32,2048]{1,0:T(8,128)(2,1)} custom-call(bf16[32,2048]{1,0:T(8,128)(2,1)} %latents_in.1, f32[1,2048]{1,0:T(1,128)} %sample_vector_in.1, bf16[64,2048]{1,0:T(8,128)(2,1)} %context_in.1, f32[1,2048]{1,0:T(1,128)} %context_vector_in.1, f32[1,2048]{1,0:T(1,128)} %bitcast.5, bf16[2048,384]{1,0:T(8,128)(2,1)} %modulator.1, ...), custom_call_target="tpu_custom_call" | custom-call | tf_op jit(solution)/shard_map/pallas_call | solution.py:695
  67.2 1.6 %copy.17 = bf16[32,2048]{1,0:T(8,128)(2,1)} copy(bf16[32,2048]{1,0:T(8,128)(2,1)} %shard_map.145) | data formatting | bytes 262144
where the time goes:
time: 68.9 us; the launch traced here: 68.8 us
  Pallas kernels  67.2 us (98%)
  local copies, waits for them, and re-layouts  1.57 us (2%)
    pallas_call x1, Pallas kernels, per_device(): pl.pallas_call(functools.partial(kernel, n_sp, n_tp), out_shape=jax.Shape...  67.2 us
    unnamed x1, local copies, waits for them, and re-layouts  1.57 us

commit v1 on v0

v1 whole, which is shorter than its diff:
```python
import functools

import jax
import jax.numpy as jnp
from jax import lax
from jax.experimental import pallas as pl
from jax.experimental.pallas import tpu as pltpu
from jax.sharding import PartitionSpec as P

DK = 128
BLOCK = 64
CTX_LIFT = 4
EPS = 1e-06
SHARP = 16.0
F32 = jnp.float32
BF16 = jnp.bfloat16
MESH = pl.DeviceIdType.MESH


def dot(a, b):
    return jnp.dot(a, b, preferred_element_type=F32)


def dot_nt(a, b):
    return lax.dot_general(a, b, (((1,), (1,)), ((), ())), preferred_element_type=F32)


def dot_tn(a, b):
    return lax.dot_general(a, b, (((0,), (0,)), ((), ())), preferred_element_type=F32)


def sums(mask, values):
    high = values.astype(BF16)
    low = (values - high.astype(F32)).astype(BF16)
    width = values.shape[1]
    both = dot(mask.astype(F32).astype(BF16), jnp.concatenate([high, low], axis=1))
    return both[:, :width] + both[:, width:]


def log_sigmoid(x):
    return jnp.minimum(x, 0.0) - jnp.log1p(jnp.exp(-jnp.abs(x)))


def kernel(
    n_sp,
    n_tp,
    latents_in,
    sample_vector_in,
    context_in,
    context_vector_in,
    norm_gain_in,
    modulator,
    query_weight,
    key_weight,
    value_weight,
    decay_down_in,
    decay_up_in,
    decay_bias_in,
    decay_extra_in,
    head_gain_in,
    out_weight,
    out,
    latents,
    sample_vector,
    context,
    context_vector,
    norm_gain,
    decay_down,
    decay_up,
    decay_bias,
    decay_extra,
    head_gain,
    mod_w,
    mods,
    lat,
    outer_context,
    extras,
    hid,
    wk,
    wv,
    wq,
    wo,
    acc_k,
    acc_v,
    acc_q,
    tots,
    key_rows,
    c_state,
    l_state,
    f_out,
    f_in,
    g_out,
    g_in,
    state,
    normed,
    part,
    rs,
    loc_sem,
    mt_s,
    mt_r,
    ms_s,
    ms_r,
    lat_s,
    lat_r,
    lo_s,
    lo_r,
    cx_s,
    cx_r,
    up_s,
    up_r,
    w_s,
    w_r,
    p_s,
    p_r,
    tt_s,
    tt_r,
    f_s,
    f_r,
    g_s,
    g_r,
    o_s,
    o_r,
    rs_s,
    rs_r,
):
    s = lax.axis_index("sp")
    t = lax.axis_index("tp")
    d = lax.axis_index("dp")
    h = lax.rem(d, 2)
    mate = d + 1 - 2 * h
    n_dev = n_sp * n_tp
    me = s * n_tp + t
    n_pairs = n_sp // 2
    pair = s // 2
    pos = lax.rem(s, 2)
    partner = s + 1 - 2 * pos
    is_worker = pos == 1 - s // n_pairs
    is_outer = pos == s // n_pairs
    rows, width = latents.shape
    ctx_rows = context.shape[0]
    length = rows * n_tp
    lat_all = 2 * length
    total = hid.shape[1]
    depth = hid.shape[2]
    half = depth // 2
    heads = decay_bias.shape[1] // DK
    dv = head_gain.shape[1]
    rank = decay_up.shape[1]
    span_t = width // n_tp

    def remote(src, dst, send, recv, device):
        return pltpu.make_async_remote_copy(
            src_ref=src,
            dst_ref=dst,
            send_sem=send,
            recv_sem=recv,
            device_id=device,
            device_id_type=MESH,
        )

    def worker_of(p):
        return 2 * p + 1 - p // (n_pairs // 2)

    def tp_peer(k):
        return lax.rem(t + k, n_tp)

    def tp_from(k):
        return lax.rem(t - k + n_tp, n_tp)

    def sp_peer(k):
        return lax.rem(s + k, n_sp)

    def sp_from(k):
        return lax.rem(s - k + n_sp, n_sp)

    weights = ((key_weight, wk), (value_weight, wv), (query_weight, wq))
    local = [pltpu.make_async_copy(modulator, mod_w, loc_sem.at[0])]
    for m, (source, slots) in enumerate(weights):
        for i in range(2):
            local.append(
                pltpu.make_async_copy(
                    source.at[pl.ds(i * half, half)], slots.at[s, i], loc_sem.at[1 + 2 * m + i]
                )
            )
    local.append(pltpu.make_async_copy(out_weight, wo, loc_sem.at[7]))
    barrier = pltpu.get_barrier_semaphore()
    for k in range(1, n_tp):
        pl.semaphore_signal(barrier, inc=1, device_id={"tp": tp_peer(k)}, device_id_type=MESH)
    for k in range(1, n_sp):
        pl.semaphore_signal(barrier, inc=1, device_id={"sp": sp_peer(k)}, device_id_type=MESH)
    pl.semaphore_signal(barrier, inc=1, device_id={"dp": mate}, device_id_type=MESH)
    small = [
        pltpu.make_async_copy(source, target, loc_sem.at[8 + i])
        for i, (source, target) in enumerate(
            (
                (sample_vector_in, sample_vector),
                (context_vector_in, context_vector),
                (latents_in, latents),
                (context_in, context),
                (decay_extra_in, decay_extra),
                (norm_gain_in, norm_gain),
                (decay_down_in, decay_down),
                (decay_up_in, decay_up),
                (decay_bias_in, decay_bias),
                (head_gain_in, head_gain),
            )
        )
    ]
    for copy in small[:5] + local[:1] + small[5:] + local[1:]:
        copy.start()
    small[2].wait()
    small[3].wait()
    small[4].wait()
    pl.semaphore_wait(barrier, n_tp + n_sp - 1)

    def inner():
        return jnp.logical_and(s >= 1, s <= n_sp - 2)

    def onward(r):
        return s + 1 <= n_sp - 2 if r == 0 else s - 1 >= 1

    def exists(r, j):
        return jnp.logical_and(inner(), s - j >= 0 if r == 0 else s + j < n_sp)

    def origin_of(r, j):
        return s - j if r == 0 else s + j

    def ring_copy(m, r, j, first=False):
        source, slots = weights[m]
        origin = origin_of(r, j)
        src = source.at[pl.ds(h * half, half)] if first else slots.at[origin, h]
        target = s + 1 if r == 0 else s - 1
        return remote(src, slots.at[origin, h], w_s.at[m, r, j], w_r.at[m, r, j], {"sp": target})

    def ring_arrival(m, r, j):
        view = weights[m][1].at[origin_of(r, j), h]
        return remote(view, view, w_s.at[m, r, j - 1], w_r.at[m, r, j - 1], {"sp": s})

    def mate_copy(m, r, j, side):
        view = weights[m][1].at[origin_of(r, j), side]
        return remote(view, view, p_s.at[m, r, j - 1], p_r.at[m, r, j - 1], {"dp": mate})

    def send_own(m):
        for r in range(2):

            @pl.when(onward(r))
            def _():
                ring_copy(m, r, 0, True).start()

    def relay(m, j, share):
        for r in range(2):

            @pl.when(exists(r, j))
            def _():
                ring_arrival(m, r, j).wait_recv()

                @pl.when(onward(r))
                def _():
                    ring_copy(m, r, j).start()

                if share:
                    mate_copy(m, r, j, h).start()

    def whole(slots, o):
        return slots[o].reshape(depth, slots.shape[3])

    def multiply(m, j, acc, count):
        slots = weights[m][1]
        for r in range(2):

            @pl.when(exists(r, j))
            def _():
                origin = origin_of(r, j)
                mate_copy(m, r, j, 1 - h).wait_recv()
                acc[...] += dot(hid[origin, 0:count], whole(slots, origin))

    def lat_copy(k):
        return remote(latents, lat.at[pos, t], lat_s.at[0, k], lat_r.at[0, k], {"tp": tp_peer(k)})

    def lat_arrival(k):
        view = lat.at[pos, tp_from(k)]
        return remote(view, view, lat_s.at[0, k], lat_r.at[0, k], {"tp": t})

    def outer_lat():
        return remote(latents, lat.at[pos, t], lo_s, lo_r, {"sp": partner})

    def outer_lat_arrival():
        view = lat.at[1 - pos, t]
        return remote(view, view, lo_s, lo_r, {"sp": s})

    def lat_relay(k, owner, to):
        view = lat.at[1 - pos, owner]
        return remote(view, view, lat_s.at[1, k], lat_r.at[1, k], {"tp": to})

    def ctx_cols(owner):
        return pl.ds(pl.multiple_of(owner * span_t, span_t), span_t)

    def ctx_copy():
        return remote(
            context.at[:, ctx_cols(t)],
            outer_context.at[:, ctx_cols(t)],
            cx_s.at[0],
            cx_r.at[0],
            {"sp": partner},
        )

    def ctx_relay(k, owner, to):
        view = outer_context.at[:, ctx_cols(owner)]
        return remote(view, view, cx_s.at[k], cx_r.at[k], {"tp": to})

    def extra_copy():
        return remote(decay_extra, extras.at[pos], up_s, up_r, {"sp": partner})

    def extra_arrival():
        view = extras.at[1 - pos]
        return remote(view, view, up_s, up_r, {"sp": s})

    @pl.when(is_outer)
    def _():
        outer_lat().start()
        extra_copy().start()
        ctx_copy().start()
        for m in range(3):
            send_own(m)

    @pl.when(is_worker)
    def _():
        for k in range(1, n_tp):
            lat_copy(k).start()
        send_own(0)
        send_own(1)

    small[0].wait()
    small[1].wait()
    is_first = lax.broadcasted_iota(jnp.int32, (16, width), 0) == 0
    vectors = jnp.where(is_first, sample_vector[...], context_vector[...])
    conditions = (vectors / (1.0 + jnp.exp(-vectors))).astype(BF16)
    local[0].wait()
    mods[me] = dot(conditions, mod_w[...])[0:2]

    def mod_tp(k, owner, to):
        view = mods.at[s * n_tp + owner]
        return remote(view, view, mt_s.at[k], mt_r.at[k], {"tp": to})

    def mod_sp(k, owner, to):
        view = mods.at[pl.ds(owner * n_tp, n_tp)]
        return remote(view, view, ms_s.at[k], ms_r.at[k], {"sp": to})

    for k in range(1, n_tp):
        mod_tp(k, t, tp_peer(k)).start()
    for k in range(1, n_tp):
        mod_tp(k, tp_from(k), t).wait_recv()
    for k in range(1, n_sp):
        mod_sp(k, s, sp_peer(k)).start()
    for copy in small[5:]:
        copy.wait()

    def modulation_now():
        for k in range(1, n_sp):
            mod_sp(k, sp_from(k), s).wait_recv()

    def mod_part(i):
        return jnp.concatenate([mods[j] for j in range(n_dev)], axis=1)[
            :, i * width : (i + 1) * width
        ]

    def tot_copy(k, owner, to):
        view = tots.at[owner]
        return remote(view, view, tt_s.at[k], tt_r.at[k], {"sp": to})

    def has_pred(z):
        return pair > 0 if z == 0 else pair < n_pairs - 1

    def has_succ(z):
        return pair < n_pairs - 1 if z == 0 else pair > 0

    def lone(a, b):
        return jnp.logical_and(a, jnp.logical_not(b))

    def f_copy(z, g):
        to = worker_of(pair + 1) if z == 0 else worker_of(pair - 1)
        return remote(f_out.at[z, g], f_in.at[z, g], f_s.at[z, g], f_r.at[z, g], {"sp": to})

    def g_copy(z, g):
        to = worker_of(pair - 1) if z == 0 else worker_of(pair + 1)
        return remote(g_out.at[z, g], g_in.at[z, g], g_s.at[z, g], g_r.at[z, g], {"sp": to})

    def o_copy(g, where, to):
        view = normed.at[where, g]
        return remote(view, view, o_s.at[g], o_r.at[g], {"sp": to})

    def work():
        outer_lat_arrival().wait_recv()
        for k in range(1, n_tp):
            lat_relay(k, t, tp_peer(k)).start()
        remote(
            outer_context.at[:, ctx_cols(t)],
            outer_context.at[:, ctx_cols(t)],
            cx_s.at[0],
            cx_r.at[0],
            {"sp": s},
        ).wait_recv()
        for k in range(1, n_tp):
            ctx_relay(k, t, tp_peer(k)).start()
        relay(0, 1, True)
        send_own(2)

        lat[pos, t] = latents[...]
        for k in range(1, n_tp):
            lat_arrival(k).wait_recv()
        modulation_now()
        shift = mod_part(0)
        scale = mod_part(1)

        def modulated(x, row):
            x = x.astype(F32)
            x = x * lax.rsqrt(jnp.mean(x * x, axis=-1, keepdims=True) + EPS) * norm_gain[...]
            return (x * (1.0 + scale[row : row + 1]) + shift[row : row + 1]).astype(BF16)

        piece = min(32, ctx_rows)

        def put(x, at):
            count = x.shape[0]
            at = pl.multiple_of(at, piece)
            for o in range(n_sp):
                hid[o, pl.ds(at, count)] = x[:, o * depth : (o + 1) * depth]

        for i in range(n_tp):
            put(modulated(lat[pos, i], 0), pos * length + i * rows)
        for i in range(ctx_rows // piece):
            put(
                modulated(context[i * piece : (i + 1) * piece], 1),
                lat_all + pos * ctx_rows + i * piece,
            )
        for k in range(1, n_tp):
            lat_relay(k, tp_from(k), t).wait_recv()
        for i in range(n_tp):
            put(modulated(lat[1 - pos, i], 0), (1 - pos) * length + i * rows)
        for k in range(1, n_tp):
            ctx_relay(k, tp_from(k), t).wait_recv()
        for i in range(ctx_rows // piece):
            put(
                modulated(outer_context[i * piece : (i + 1) * piece], 1),
                lat_all + (1 - pos) * ctx_rows + i * piece,
            )

        low = dot_nt(hid[0], decay_down[:, 0:depth])
        for o in range(1, n_sp):
            low = low + dot_nt(hid[o], decay_down[:, o * depth : (o + 1) * depth])
        low = low.astype(BF16)
        relay(1, 1, True)

        def log_decays(z):
            x = dot(low[:, z * rank : (z + 1) * rank], decay_up[z]) + decay_bias[z : z + 1]
            return log_sigmoid(x) / SHARP

        row_id = lax.broadcasted_iota(jnp.int32, (lat_all, lat_all), 0)
        col_id = lax.broadcasted_iota(jnp.int32, (lat_all, lat_all), 1)
        same = row_id // BLOCK == col_id // BLOCK
        within_mask = [same & (col_id <= row_id), same & (col_id >= row_id)]
        extras[pos] = decay_extra[...]
        extra_arrival().wait_recv()

        def extra_sums(z):
            columns = []
            for g in range(heads):
                line = jnp.concatenate([extras[i, z, g : g + 1, :] for i in range(2)], axis=1)
                columns.append(
                    jnp.sum(jnp.where(within_mask[z], line, 0.0), axis=1, keepdims=True)
                )
            return jnp.concatenate([jnp.broadcast_to(c, (lat_all, DK)) for c in columns], axis=1)

        decays = [log_decays(z) for z in range(2)]
        within = [sums(within_mask[z], decays[z][:lat_all]) + extra_sums(z) for z in range(2)]
        blocks = lat_all // BLOCK
        totals = [
            [within[0][(b + 1) * BLOCK - 1 : (b + 1) * BLOCK] for b in range(blocks)],
            [within[1][b * BLOCK : b * BLOCK + 1] for b in range(blocks)],
        ]
        none = jnp.zeros_like(totals[0][0])

        def between(z, lo, hi):
            value = none
            for b in range(lo, hi):
                value = value + totals[z][b]
            return value

        crow = lax.broadcasted_iota(jnp.int32, (total - lat_all, total - lat_all), 0)
        ccol = lax.broadcasted_iota(jnp.int32, (total - lat_all, total - lat_all), 1)
        after = [
            sums(ccol > crow, decays[0][lat_all:]),
            sums(ccol < crow, decays[1][lat_all:]),
        ]
        lat_total = [between(z, 0, blocks) for z in range(2)]
        ctx_total = [
            after[0][0:1] + decays[0][lat_all : lat_all + 1],
            after[1][total - lat_all - 1 :] + decays[1][total - 1 :],
        ]
        tots[pair] = jnp.concatenate(lat_total + ctx_total, axis=0)
        for k in range(1, n_pairs):
            to = lax.rem(pair + k, n_pairs)
            tot_copy(k, pair, worker_of(to)).start()

        for copy in local[1:5]:
            copy.wait()
        acc_k[...] = dot(hid[s], whole(wk, s))
        acc_v[...] = dot(hid[s], whole(wv, s))
        multiply(0, 1, acc_k, total)
        multiply(1, 1, acc_v, total)
        for k in range(1, n_pairs):
            tot_copy(k, lax.rem(pair - k + n_pairs, n_pairs), s).wait_recv()
        before = [none, none]
        suffix = [none, none]
        for u in range(n_pairs):
            line = tots[u]
            below = jnp.where(u < pair, 1.0, 0.0)
            above = jnp.where(u > pair, 1.0, 0.0)
            before[0] = before[0] + below * line[0:1]
            before[1] = before[1] + above * line[1:2]
            suffix[0] = suffix[0] + above * line[2:3]
            suffix[1] = suffix[1] + below * line[3:4]
        ctx_weight = [jnp.exp(after[z] + suffix[z]) for z in range(2)]

        def per_block(f):
            return jnp.concatenate([f(b) for b in range(blocks)], axis=0)

        def rows_of(x, b):
            return x[b * BLOCK : (b + 1) * BLOCK]

        ending = [
            jnp.exp(
                per_block(
                    lambda b: totals[0][b] - rows_of(within[0], b) + between(0, b + 1, blocks)
                )
            ),
            jnp.exp(per_block(lambda b: totals[1][b] - rows_of(within[1], b) + between(1, 0, b))),
        ]
        for j in range(2, max(n_sp - 1, 2)):
            relay(0, j, True)
            multiply(0, j, acc_k, total)
            if j == 2:
                relay(2, 1, True)
            relay(1, j, True)
            multiply(1, j, acc_v, total)
        keys = acc_k[...].astype(BF16)
        values = acc_v[...].astype(BF16)
        ckeys = keys[lat_all:].astype(F32)
        cvals = values[lat_all:]
        keys = keys[:lat_all].astype(F32)
        values = values[:lat_all]

        def columns(g, n):
            return slice(g * n, (g + 1) * n)

        for z in range(2):
            ended = (keys * ending[z]).astype(BF16)
            cended = (ckeys * ctx_weight[z]).astype(BF16)
            lift = CTX_LIFT * jnp.exp(before[z])
            lift_on = CTX_LIFT * jnp.exp(before[z] + lat_total[z])
            for g in range(heads):
                c = dot_tn(cvals[:, columns(g, dv)], cended[:, columns(g, DK)])
                g_out[z, g] = c.astype(BF16)
                own = dot_tn(values[:, columns(g, dv)], ended[:, columns(g, DK)])
                f_out[z, g] = (own + lift_on[:, columns(g, DK)] * c).astype(BF16)
                if n_pairs > 2:
                    c_state[z, g] = c
                    l_state[z, g] = own + lift_on[:, columns(g, DK)] * c
                state[z, g] = lift[:, columns(g, DK)] * c

                @pl.when(lone(has_succ(z), has_pred(z)))
                def _():
                    f_copy(z, g).start()

                @pl.when(lone(has_pred(z), has_succ(z)))
                def _():
                    g_copy(z, g).start()

        if n_pairs > 2:
            for z in range(2):

                @pl.when(jnp.logical_and(has_pred(z), has_succ(z)))
                def _():
                    for g in range(heads):
                        f_copy(z, g).wait_recv()
                        on = jnp.exp(lat_total[z])[:, columns(g, DK)]
                        f_out[z, g] = (l_state[z, g] + on * f_in[z, g].astype(F32)).astype(BF16)
                        f_copy(z, g).start()

                @pl.when(jnp.logical_and(has_pred(z), has_succ(z)))
                def _():
                    for g in range(heads):
                        g_copy(z, g).wait_recv()
                        g_out[z, g] = (c_state[z, g] + g_in[z, g].astype(F32)).astype(BF16)
                        g_copy(z, g).start()

        for z in range(2):
            close = (keys * jnp.exp(-within[z])).astype(BF16)
            near = keys * jnp.exp(per_block(lambda b: totals[z][b] - rows_of(within[z], b)))
            for i in range(blocks):
                for j in range(blocks):
                    if i == j:
                        block = rows_of(close, j)
                    elif (j < i) == (z == 0):
                        gap = between(z, min(i, j) + 1, max(i, j))
                        block = (rows_of(near, j) * jnp.exp(gap)).astype(BF16)
                    else:
                        block = jnp.zeros((BLOCK, heads * DK), BF16)
                    key_rows[z, i, j * BLOCK : (j + 1) * BLOCK] = block
        reach = [jnp.exp(within[z]) for z in range(2)]
        lifted_by = [
            jnp.exp(per_block(lambda b: rows_of(within[0], b) + between(0, 0, b))),
            jnp.exp(per_block(lambda b: rows_of(within[1], b) + between(1, b + 1, blocks))),
        ]

        for copy in local[5:7]:
            copy.wait()
        acc_q[...] = dot(hid[s, 0:lat_all], whole(wq, s))
        for j in range(1, max(n_sp - 1, 2)):
            if j > 1:
                relay(2, j, True)
            multiply(2, j, acc_q, lat_all)
        queries = acc_q[...].astype(BF16).astype(F32)

        query_dec = [(queries * reach[z]).astype(BF16) for z in range(2)]
        lifted = [(queries * lifted_by[z]).astype(BF16) for z in range(2)]
        masks = [col_id <= row_id, col_id >= row_id]
        for z in range(2):
            lift = CTX_LIFT * jnp.exp(before[z])

            @pl.when(has_pred(z))
            def _():
                for g in range(heads):
                    if n_pairs == 2:
                        f_copy(z, g).wait_recv()
                    else:

                        @pl.when(jnp.logical_not(has_succ(z)))
                        def _():
                            f_copy(z, g).wait_recv()

                    state[z, g] += f_in[z, g].astype(F32)

            @pl.when(has_succ(z))
            def _():
                for g in range(heads):
                    if n_pairs == 2:
                        g_copy(z, g).wait_recv()
                    else:

                        @pl.when(jnp.logical_not(has_pred(z)))
                        def _():
                            g_copy(z, g).wait_recv()

                    state[z, g] += lift[:, columns(g, DK)] * g_in[z, g].astype(F32)

        for g in range(heads):
            cs = columns(g, DK)
            lines = []
            for i in range(blocks):
                line = 0.0
                for z in range(2):
                    score = dot_nt(rows_of(query_dec[z], i)[:, cs], key_rows[z, i, :, cs])
                    line = line + jnp.where(rows_of(masks[z], i), score, 0.0)
                lines.append(line.astype(BF16))
            mixed = dot(jnp.concatenate(lines, axis=0), values[:, columns(g, dv)])
            for z in range(2):
                mixed = mixed + dot_nt(lifted[z][:, cs], state[z, g].astype(BF16))
            by = lax.rsqrt(jnp.mean(mixed * mixed, axis=-1, keepdims=True) + EPS)
            result = (mixed * by * head_gain[...]).astype(BF16)
            for i in range(2):
                normed[i, g] = result[i * length : (i + 1) * length]
            o_copy(g, 1 - pos, partner).start()

    pl.when(is_worker)(work)

    @pl.when(is_outer)
    def _():
        for copy in local[1:7]:
            copy.wait()
        for m in (0, 1):
            relay(m, 1, False)
        for j in range(2, n_sp - 1):
            relay(0, j, False)
            if j == 2:
                relay(2, 1, False)
            relay(1, j, False)
        for j in range(2, n_sp - 1):
            relay(2, j, False)
        modulation_now()
        for g in range(heads):
            o_copy(g, pos, s).wait_recv()

    gate = mod_part(2)[0:1]
    local[7].wait()
    chunks = rs_s.shape[1]
    span = width // chunks
    rs_copies = []
    for c in range(chunks):
        cols = slice(c * span, (c + 1) * span)
        product = dot(normed[pos, 0], wo[0:dv, cols])
        for g in range(1, heads):
            product = product + dot(normed[pos, g], wo[g * dv : (g + 1) * dv, cols])
        product = product.astype(BF16)
        for i in range(n_tp):
            part[i, :, cols] = product[i * rows : (i + 1) * rows]
        for k in range(1, n_tp):
            to = tp_peer(k)
            copy = remote(
                part.at[to, :, pl.ds(c * span, span)],
                rs.at[k, :, pl.ds(c * span, span)],
                rs_s.at[k, c],
                rs_r.at[k, c],
                {"tp": to},
            )
            copy.start()
            rs_copies.append(copy)
    for c in range(chunks):
        cols = slice(c * span, (c + 1) * span)
        summed = part[t, :, cols].astype(F32)
        for k in range(1, n_tp):
            rs_copies[c * (n_tp - 1) + k - 1].wait_recv()
            summed = summed + rs[k, :, cols].astype(F32)
        projected = summed.astype(BF16).astype(F32)
        out[:, cols] = (latents[:, cols].astype(F32) + gate[:, cols] * projected).astype(BF16)

    for copy in rs_copies:
        copy.wait_send()
    for k in range(1, n_tp):
        mod_tp(k, t, tp_peer(k)).wait_send()
    for k in range(1, n_sp):
        mod_sp(k, s, sp_peer(k)).wait_send()

    @pl.when(is_outer)
    def _():
        outer_lat().wait_send()
        extra_copy().wait_send()
        ctx_copy().wait_send()

    @pl.when(is_worker)
    def _():
        for k in range(1, n_tp):
            lat_copy(k).wait_send()
            lat_relay(k, t, tp_peer(k)).wait_send()
            ctx_relay(k, t, tp_peer(k)).wait_send()
        for k in range(1, n_pairs):
            tot_copy(k, pair, s).wait_send()
        for g in range(heads):
            o_copy(g, 1 - pos, partner).wait_send()
            for z in range(2):

                @pl.when(has_succ(z))
                def _():
                    f_copy(z, g).wait_send()

                @pl.when(has_pred(z))
                def _():
                    g_copy(z, g).wait_send()

    for m in range(3):
        for r in range(2):

            @pl.when(onward(r))
            def _():
                ring_copy(m, r, 0, True).wait_send()

            for j in range(1, n_sp - 1):

                @pl.when(exists(r, j))
                def _():
                    @pl.when(onward(r))
                    def _():
                        ring_copy(m, r, j).wait_send()

                    @pl.when(is_worker)
                    def _():
                        mate_copy(m, r, j, h).wait_send()


def per_device(n_sp, n_tp, *args):
    (latents, sv, context, cv, gain, modulator, wq, wk, wv, down, up, bias, extra, hg, wo) = args
    rows, width = latents.shape
    ctx_rows = context.shape[0]
    n_dev = n_sp * n_tp
    n_pairs = n_sp // 2
    length = rows * n_tp
    total = 2 * (length + ctx_rows)
    depth = wq.shape[0]
    kw, vw = wk.shape[1], wv.shape[1]
    heads = bias.shape[1] // DK
    dv = hg.shape[0]
    chunks = 4
    vmem = pl.BlockSpec(memory_space=pltpu.VMEM)
    hbm = pl.BlockSpec(memory_space=pl.ANY)
    dma = pltpu.SemaphoreType.DMA
    states = (2, heads, dv, DK)
    chained = states if n_pairs > 2 else (2, heads, 8, DK)
    scratch = [
        pltpu.VMEM(latents.shape, BF16),
        pltpu.VMEM(sv.shape, F32),
        pltpu.VMEM(context.shape, BF16),
        pltpu.VMEM(cv.shape, F32),
        pltpu.VMEM((1, width), F32),
        pltpu.VMEM(down.shape[::-1], BF16),
        pltpu.VMEM(up.shape, BF16),
        pltpu.VMEM(bias.shape, F32),
        pltpu.VMEM((2, heads, length), F32),
        pltpu.VMEM((1, dv), F32),
        pltpu.VMEM(modulator.shape, BF16),
        pltpu.VMEM((n_dev, 2, modulator.shape[1]), F32),
        pltpu.VMEM((2, n_tp, rows, width), BF16),
        pltpu.VMEM((ctx_rows, width), BF16),
        pltpu.VMEM((2, 2, heads, length), F32),
        pltpu.VMEM((n_sp, total, depth), BF16),
        pltpu.VMEM((n_sp, 2, depth // 2, kw), BF16),
        pltpu.VMEM((n_sp, 2, depth // 2, vw), BF16),
        pltpu.VMEM((n_sp, 2, depth // 2, kw), BF16),
        pltpu.VMEM(wo.shape, BF16),
        pltpu.VMEM((total, kw), F32),
        pltpu.VMEM((total, vw), F32),
        pltpu.VMEM((2 * length, kw), F32),
        pltpu.VMEM((n_pairs, 4, kw), F32),
        pltpu.VMEM((2, 2 * length // BLOCK, 2 * length, kw), BF16),
        pltpu.VMEM(chained, F32),
        pltpu.VMEM(chained, F32),
        pltpu.VMEM(states, BF16),
        pltpu.VMEM(states, BF16),
        pltpu.VMEM(states, BF16),
        pltpu.VMEM(states, BF16),
        pltpu.VMEM(states, F32),
        pltpu.VMEM((2, heads, length, dv), BF16),
        pltpu.VMEM((n_tp, rows, width), BF16),
        pltpu.VMEM((n_tp, rows, width), BF16),
        dma((18,)),
        dma((n_tp,)),
        dma((n_tp,)),
        dma((n_sp,)),
        dma((n_sp,)),
        dma((2, n_tp)),
        dma((2, n_tp)),
        dma,
        dma,
        dma((n_tp,)),
        dma((n_tp,)),
        dma,
        dma,
        dma((3, 2, n_sp)),
        dma((3, 2, n_sp)),
        dma((3, 2, n_sp)),
        dma((3, 2, n_sp)),
        dma((n_pairs,)),
        dma((n_pairs,)),
        dma((2, heads)),
        dma((2, heads)),
        dma((2, heads)),
        dma((2, heads)),
        dma((heads,)),
        dma((heads,)),
        dma((n_tp, chunks)),
        dma((n_tp, chunks)),
    ]
    return pl.pallas_call(
        functools.partial(kernel, n_sp, n_tp),
        out_shape=jax.ShapeDtypeStruct(latents.shape, BF16),
        in_specs=[hbm] * 15,
        out_specs=vmem,
        scratch_shapes=scratch,
        compiler_params=pltpu.CompilerParams(
            collective_id=0, has_side_effects=True, vmem_limit_bytes=56 * 1024 * 1024
        ),
    )(
        latents,
        sv,
        context,
        cv,
        gain.reshape(1, -1),
        modulator,
        wq,
        wk,
        wv,
        down.T,
        up,
        bias,
        extra.transpose(0, 2, 1),
        hg.reshape(1, -1),
        wo,
    )


def solution(mesh):
    placed = (
        P(("dp", "sp", "tp"), None),
        P("dp", None),
        P(("dp", "sp"), None),
        P(),
        P(),
        P(None, ("sp", "tp")),
        P("sp", "tp"),
        P("sp", "tp"),
        P("sp", "tp"),
        P(),
        P(None, None, "tp"),
        P(None, "tp"),
        P(None, ("dp", "sp"), "tp"),
        P(),
        P("tp", None),
    )
    return jax.shard_map(
        functools.partial(per_device, mesh.shape["sp"], mesh.shape["tp"]),
        mesh=mesh,
        in_specs=placed,
        out_specs=P(("dp", "sp", "tp"), None),
        check_vma=False,
    )
```

time: 68.9 us -> 59.5 us (0.86)
  Pallas kernels: 67.2 us -> 57.8 us
    pallas_call x1, Pallas kernels: 67.2 us -> 57.8 us  [per_device(): pl.pallas_call(functools.partial(kernel, n_sp, n_tp), out_shape=jax.Shape...]
where the time goes in v1:
time: 59.5 us; the launch traced here: 59.3 us
  Pallas kernels  57.8 us (97%)
  local copies, waits for them, and re-layouts  1.57 us (3%)
    pallas_call x1, Pallas kernels, per_device(): pl.pallas_call(functools.partial(kernel, n_sp, n_tp), out_shape=jax.Shape...  57.8 us
    unnamed x1, local copies, waits for them, and re-layouts  1.57 us

profile of v1, /device:TPU:0, one launch (start us, length us, event | category | flops | bytes accessed | tf_op | source)
XLA Modules:
  0.0 59.3 jit_solution(18050069251419433722)
XLA Ops:
  0.0 57.8 %shard_map.145 = bf16[32,2048]{1,0:T(8,128)(2,1)} custom-call(bf16[32,2048]{1,0:T(8,128)(2,1)} %latents_in.1, f32[1,2048]{1,0:T(1,128)} %sample_vector_in.1, bf16[64,2048]{1,0:T(8,128)(2,1)} %context_in.1, f32[1,2048]{1,0:T(1,128)} %context_vector_in.1, f32[1,2048]{1,0:T(1,128)} %bitcast.5, bf16[2048,384]{1,0:T(8,128)(2,1)} %modulator.1, ...), custom_call_target="tpu_custom_call" | custom-call | tf_op jit(solution)/shard_map/pallas_call | solution.py:861
  57.8 1.6 %copy.17 = bf16[32,2048]{1,0:T(8,128)(2,1)} copy(bf16[32,2048]{1,0:T(8,128)(2,1)} %shard_map.145) | data formatting | bytes 262144

commit v2 on v1

--- a/solution.py
+++ b/solution.py
@@ -41,7 +41,7 @@
     return jnp.minimum(x, 0.0) - jnp.log1p(jnp.exp(-jnp.abs(x)))
 
 
-def kernel(
+def chain_kernel(
     n_sp,
     n_tp,
     latents_in,
@@ -85,6 +85,7 @@
     acc_q,
     tots,
     key_rows,
+    query_rows,
     c_state,
     l_state,
     f_out,
@@ -434,6 +435,7 @@
             )
         for k in range(1, n_tp):
             lat_relay(k, tp_from(k), t).wait_recv()
+        relay(1, 1, True)
         for i in range(n_tp):
             put(modulated(lat[1 - pos, i], 0), (1 - pos) * length + i * rows)
         for k in range(1, n_tp):
@@ -448,7 +450,7 @@
         for o in range(1, n_sp):
             low = low + dot_nt(hid[o], decay_down[:, o * depth : (o + 1) * depth])
         low = low.astype(BF16)
-        relay(1, 1, True)
+        relay(2, 1, True)
 
         def log_decays(z):
             x = dot(low[:, z * rank : (z + 1) * rank], decay_up[z]) + decay_bias[z : z + 1]
@@ -538,8 +540,6 @@
         for j in range(2, max(n_sp - 1, 2)):
             relay(0, j, True)
             multiply(0, j, acc_k, total)
-            if j == 2:
-                relay(2, 1, True)
             relay(1, j, True)
             multiply(1, j, acc_v, total)
         keys = acc_k[...].astype(BF16)
@@ -621,9 +621,39 @@
             multiply(2, j, acc_q, lat_all)
         queries = acc_q[...].astype(BF16).astype(F32)
 
-        query_dec = [(queries * reach[z]).astype(BF16) for z in range(2)]
-        lifted = [(queries * lifted_by[z]).astype(BF16) for z in range(2)]
-        masks = [col_id <= row_id, col_id >= row_id]
+        for z in range(2):
+            near_rows = (queries * reach[z]).astype(BF16)
+            far_rows = (queries * lifted_by[z]).astype(BF16)
+            for b in range(blocks):
+                query_rows[0, z, b] = rows_of(near_rows, b)
+                query_rows[1, z, b] = rows_of(far_rows, b)
+        turn = blocks // 2
+        row_in = lax.broadcasted_iota(jnp.int32, (BLOCK, lat_all), 0)
+        col_in = lax.broadcasted_iota(jnp.int32, (BLOCK, lat_all), 1)
+
+        def inside(where, g):
+            lines = []
+            for b in range(turn):
+                i = where * turn + b
+                ids = row_in + i * BLOCK
+                masks = [col_in <= ids, col_in >= ids]
+                line = 0.0
+                for z in range(2):
+                    score = dot_nt(
+                        query_rows[0, z, i, :, columns(g, DK)], key_rows[z, i, :, columns(g, DK)]
+                    )
+                    line = line + jnp.where(masks[z], score, 0.0)
+                lines.append(line.astype(BF16))
+            return dot(jnp.concatenate(lines, axis=0), values[:, columns(g, dv)])
+
+        def finish(where, g, mixed):
+            for z in range(2):
+                rows_z = query_rows[1, z, pl.ds(where * turn, turn), :, columns(g, DK)]
+                mixed = mixed + dot_nt(rows_z.reshape(length, DK), state[z, g].astype(BF16))
+            by = lax.rsqrt(jnp.mean(mixed * mixed, axis=-1, keepdims=True) + EPS)
+            normed[where, g] = (mixed * by * head_gain[...]).astype(BF16)
+
+        first = [inside(1 - pos, g) for g in range(heads)]
         for z in range(2):
             lift = CTX_LIFT * jnp.exp(before[z])
 
@@ -654,22 +684,10 @@
                     state[z, g] += lift[:, columns(g, DK)] * g_in[z, g].astype(F32)
 
         for g in range(heads):
-            cs = columns(g, DK)
-            lines = []
-            for i in range(blocks):
-                line = 0.0
-                for z in range(2):
-                    score = dot_nt(rows_of(query_dec[z], i)[:, cs], key_rows[z, i, :, cs])
-                    line = line + jnp.where(rows_of(masks[z], i), score, 0.0)
-                lines.append(line.astype(BF16))
-            mixed = dot(jnp.concatenate(lines, axis=0), values[:, columns(g, dv)])
-            for z in range(2):
-                mixed = mixed + dot_nt(lifted[z][:, cs], state[z, g].astype(BF16))
-            by = lax.rsqrt(jnp.mean(mixed * mixed, axis=-1, keepdims=True) + EPS)
-            result = (mixed * by * head_gain[...]).astype(BF16)
-            for i in range(2):
-                normed[i, g] = result[i * length : (i + 1) * length]
+            finish(1 - pos, g, first[g])
             o_copy(g, 1 - pos, partner).start()
+        for g in range(heads):
+            finish(pos, g, inside(pos, g))
 
     pl.when(is_worker)(work)
 
@@ -677,12 +695,10 @@
     def _():
         for copy in local[1:7]:
             copy.wait()
-        for m in (0, 1):
+        for m in range(3):
             relay(m, 1, False)
         for j in range(2, n_sp - 1):
             relay(0, j, False)
-            if j == 2:
-                relay(2, 1, False)
             relay(1, j, False)
         for j in range(2, n_sp - 1):
             relay(2, j, False)
@@ -776,7 +792,7 @@
                         mate_copy(m, r, j, h).wait_send()
 
 
-def per_device(n_sp, n_tp, *args):
+def chain_per_device(n_sp, n_tp, *args):
     (latents, sv, context, cv, gain, modulator, wq, wk, wv, down, up, bias, extra, hg, wo) = args
     rows, width = latents.shape
     ctx_rows = context.shape[0]
@@ -820,6 +836,7 @@
         pltpu.VMEM((2 * length, kw), F32),
         pltpu.VMEM((n_pairs, 4, kw), F32),
         pltpu.VMEM((2, 2 * length // BLOCK, 2 * length, kw), BF16),
+        pltpu.VMEM((2, 2, 2 * length // BLOCK, BLOCK, kw), BF16),
         pltpu.VMEM(chained, F32),
         pltpu.VMEM(chained, F32),
         pltpu.VMEM(states, BF16),
@@ -859,6 +876,755 @@
         dma((n_tp, chunks)),
     ]
     return pl.pallas_call(
+        functools.partial(chain_kernel, n_sp, n_tp),
+        out_shape=jax.ShapeDtypeStruct(latents.shape, BF16),
+        in_specs=[hbm] * 15,
+        out_specs=vmem,
+        scratch_shapes=scratch,
+        compiler_params=pltpu.CompilerParams(
+            collective_id=0, has_side_effects=True, vmem_limit_bytes=56 * 1024 * 1024
+        ),
+    )(
+        latents,
+        sv,
+        context,
+        cv,
+        gain.reshape(1, -1),
+        modulator,
+        wq,
+        wk,
+        wv,
+        down.T,
+        up,
+        bias,
+        extra.transpose(0, 2, 1),
+        hg.reshape(1, -1),
+        wo,
+    )
+
+
+def kernel(
+    n_sp,
+    n_tp,
+    latents_in,
+    sample_vector_in,
+    context_in,
+    context_vector_in,
+    norm_gain_in,
+    modulator,
+    query_weight,
+    key_weight,
+    value_weight,
+    decay_down_in,
+    decay_up_in,
+    decay_bias_in,
+    decay_extra_in,
+    head_gain_in,
+    out_weight,
+    out,
+    latents,
+    sample_vector,
+    context,
+    context_vector,
+    norm_gain,
+    decay_down,
+    decay_up,
+    decay_bias,
+    decay_extra,
+    head_gain,
+    mod_w,
+    mods,
+    lat,
+    ctx,
+    extras,
+    hid,
+    wk,
+    wv,
+    wq,
+    wo,
+    acc_k,
+    acc_v,
+    acc_q,
+    key_rows,
+    o_out,
+    normed,
+    part,
+    rs,
+    loc_sem,
+    mt_s,
+    mt_r,
+    ms_s,
+    ms_r,
+    lo_s,
+    lo_r,
+    cx_s,
+    cx_r,
+    ex_s,
+    ex_r,
+    em_s,
+    em_r,
+    lp_s,
+    lp_r,
+    cp_s,
+    cp_r,
+    hd_s,
+    hd_r,
+    w_s,
+    w_r,
+    o_s,
+    o_r,
+    rs_s,
+    rs_r,
+):
+    s = lax.axis_index("sp")
+    t = lax.axis_index("tp")
+    d = lax.axis_index("dp")
+    h = lax.rem(d, 2)
+    mate = d + 1 - 2 * h
+    n_dev = n_sp * n_tp
+    me = s * n_tp + t
+    first_plane = n_sp // 2 - 1
+    last_plane = n_sp // 2
+    side = s - first_plane
+    target = first_plane + h
+    is_worker = jnp.logical_and(s >= first_plane, s <= last_plane)
+    is_leader = s == target
+    is_follower = jnp.logical_and(is_worker, s != target)
+    is_sender = s != target
+    rows, width = latents.shape
+    ctx_rows = context.shape[0]
+    length = rows * n_tp
+    lat_all = n_sp * length
+    total = hid.shape[1]
+    depth = hid.shape[2]
+    heads = decay_bias.shape[1] // DK
+    dv = head_gain.shape[1]
+    rank = decay_up.shape[1]
+    span_t = width // n_tp
+
+    def remote(src, dst, send, recv, device):
+        return pltpu.make_async_remote_copy(
+            src_ref=src,
+            dst_ref=dst,
+            send_sem=send,
+            recv_sem=recv,
+            device_id=device,
+            device_id_type=MESH,
+        )
+
+    def tp_peer(k):
+        return lax.rem(t + k, n_tp)
+
+    def tp_from(k):
+        return lax.rem(t - k + n_tp, n_tp)
+
+    def sp_peer(k):
+        return lax.rem(s + k, n_sp)
+
+    def sp_from(k):
+        return lax.rem(s - k + n_sp, n_sp)
+
+    def head_cols(size):
+        return pl.ds(pl.multiple_of(h * size, DK), size)
+
+    weights = ((key_weight, wk, DK), (value_weight, wv, dv), (query_weight, wq, DK))
+    own_weight = [
+        pltpu.make_async_copy(source.at[:, head_cols(size)], slots.at[s], loc_sem.at[1 + m])
+        for m, (source, slots, size) in enumerate(weights)
+    ]
+    mod_load = pltpu.make_async_copy(modulator, mod_w, loc_sem.at[0])
+    out_load = pltpu.make_async_copy(out_weight, wo, loc_sem.at[4])
+    barrier = pltpu.get_barrier_semaphore()
+    for k in range(1, n_tp):
+        pl.semaphore_signal(barrier, inc=1, device_id={"tp": tp_peer(k)}, device_id_type=MESH)
+    for k in range(1, n_sp):
+        pl.semaphore_signal(barrier, inc=1, device_id={"sp": sp_peer(k)}, device_id_type=MESH)
+    pl.semaphore_signal(barrier, inc=1, device_id={"dp": mate}, device_id_type=MESH)
+    small = [
+        pltpu.make_async_copy(source, where, loc_sem.at[8 + i])
+        for i, (source, where) in enumerate(
+            (
+                (sample_vector_in, sample_vector),
+                (context_vector_in, context_vector),
+                (latents_in, latents),
+                (context_in, context),
+                (decay_extra_in, decay_extra),
+                (norm_gain_in, norm_gain),
+                (decay_down_in, decay_down),
+                (decay_up_in, decay_up),
+                (decay_bias_in, decay_bias),
+                (head_gain_in, head_gain),
+            )
+        )
+    ]
+    for copy in small[:5] + own_weight + [mod_load] + small[5:] + [out_load]:
+        copy.start()
+    for copy in small[2:5] + own_weight:
+        copy.wait()
+    pl.semaphore_wait(barrier, n_tp + n_sp - 1)
+
+    def onward(r):
+        return s + 1 <= last_plane if r == 0 else s - 1 >= first_plane
+
+    def exists(r, j):
+        if r == 0:
+            return jnp.logical_and(s <= last_plane, s - j >= 0)
+        return jnp.logical_and(s >= first_plane, s + j < n_sp)
+
+    def origin_of(r, j):
+        return s - j if r == 0 else s + j
+
+    def ring_copy(m, r, j):
+        view = weights[m][1].at[origin_of(r, j)]
+        to = s + 1 if r == 0 else s - 1
+        return remote(view, view, w_s.at[m, r, j], w_r.at[m, r, j], {"sp": to})
+
+    def ring_arrival(m, r, j):
+        view = weights[m][1].at[origin_of(r, j)]
+        return remote(view, view, w_s.at[m, r, j - 1], w_r.at[m, r, j - 1], {"sp": s})
+
+    def relay(m, j):
+        for r in range(2):
+
+            @pl.when(exists(r, j))
+            def _():
+                ring_arrival(m, r, j).wait_recv()
+
+                @pl.when(onward(r))
+                def _():
+                    ring_copy(m, r, j).start()
+
+    def multiply(m, j, acc, count):
+        slots = weights[m][1]
+        for r in range(2):
+
+            @pl.when(exists(r, j))
+            def _():
+                origin = origin_of(r, j)
+                acc[...] += dot(hid[origin, 0:count], slots[origin])
+
+    def lat_in(b, to):
+        view = lat.at[b, t]
+        return remote(latents, view, lo_s, lo_r.at[b], {"sp": to})
+
+    def extra_in(b, to):
+        return remote(decay_extra, extras.at[b], ex_s, ex_r.at[b], {"sp": to})
+
+    def ctx_cols(owner):
+        return pl.ds(pl.multiple_of(owner * span_t, span_t), span_t)
+
+    def ctx_in(b, to):
+        return remote(
+            context.at[:, ctx_cols(t)],
+            ctx.at[b, :, ctx_cols(t)],
+            cx_s,
+            cx_r.at[b],
+            {"sp": to},
+        )
+
+    def lat_plane(b, k, owner, to):
+        view = lat.at[b, owner]
+        return remote(view, view, lp_s.at[b, k], lp_r.at[b, k], {"tp": to})
+
+    def lat_own(k):
+        return remote(latents, lat.at[s, t], lp_s.at[s, k], lp_r.at[s, k], {"tp": tp_peer(k)})
+
+    def ctx_plane(b, k, owner, to):
+        view = ctx.at[b, :, ctx_cols(owner)]
+        return remote(view, view, cp_s.at[b, k], cp_r.at[b, k], {"tp": to})
+
+    def hid_copy(i, at, count):
+        view = hid.at[:, pl.ds(pl.multiple_of(at, 16), count)]
+        return remote(view, view, hd_s.at[i], hd_r.at[i], {"dp": mate})
+
+    def lat_hid(b):
+        return hid_copy(b, b * length, length)
+
+    def ctx_hid(b):
+        return hid_copy(n_sp + b, lat_all + b * ctx_rows, ctx_rows)
+
+    def extra_mate():
+        return remote(extras, extras, em_s, em_r, {"dp": mate})
+
+    def others():
+        towards = 1 - 2 * side
+        steps = sorted(range(-first_plane, n_sp // 2 + 1), key=abs)
+        return [s + towards * step for step in steps if step]
+
+    @pl.when(is_sender)
+    def _():
+        lat_in(s, target).start()
+        extra_in(s, target).start()
+        ctx_in(s, target).start()
+
+    @pl.when(is_leader)
+    def _():
+        for k in range(1, n_tp):
+            lat_own(k).start()
+
+    for m in range(3):
+        for r in range(2):
+
+            @pl.when(onward(r))
+            def _():
+                ring_copy(m, r, 0).start()
+
+    small[0].wait()
+    small[1].wait()
+    is_first = lax.broadcasted_iota(jnp.int32, (16, width), 0) == 0
+    vectors = jnp.where(is_first, sample_vector[...], context_vector[...])
+    conditions = (vectors / (1.0 + jnp.exp(-vectors))).astype(BF16)
+    mod_load.wait()
+    mods[me] = dot(conditions, mod_w[...])[0:2]
+
+    def mod_tp(k, owner, to):
+        view = mods.at[s * n_tp + owner]
+        return remote(view, view, mt_s.at[k], mt_r.at[k], {"tp": to})
+
+    def mod_sp(k, owner, to):
+        view = mods.at[pl.ds(owner * n_tp, n_tp)]
+        return remote(view, view, ms_s.at[k], ms_r.at[k], {"sp": to})
+
+    for k in range(1, n_tp):
+        mod_tp(k, t, tp_peer(k)).start()
+    for k in range(1, n_tp):
+        mod_tp(k, tp_from(k), t).wait_recv()
+    for k in range(1, n_sp):
+        mod_sp(k, s, sp_peer(k)).start()
+    for copy in small[5:]:
+        copy.wait()
+
+    def mod_part(i):
+        return jnp.concatenate([mods[j] for j in range(n_dev)], axis=1)[
+            :, i * width : (i + 1) * width
+        ]
+
+    def mods_arrive():
+        for k in range(1, n_sp):
+            mod_sp(k, sp_from(k), s).wait_recv()
+
+    piece = min(32, ctx_rows)
+
+    def put(x, row, at):
+        count = x.shape[0]
+        x = x.astype(F32)
+        x = x * lax.rsqrt(jnp.mean(x * x, axis=-1, keepdims=True) + EPS) * norm_gain[...]
+        scale = mod_part(1)[row : row + 1]
+        shift = mod_part(0)[row : row + 1]
+        x = (x * (1.0 + scale) + shift).astype(BF16)
+        at = pl.multiple_of(at, piece)
+        for o in range(n_sp):
+            hid[o, pl.ds(at, count)] = x[:, o * depth : (o + 1) * depth]
+
+    def o_copy(b):
+        lead = jnp.where(side == h, d, mate)
+        return remote(
+            o_out.at[b], normed.at[h], o_s.at[b], o_r.at[h], {"sp": b, "dp": lead}
+        )
+
+    def o_mate():
+        return remote(o_out.at[s], normed.at[h], o_s.at[s], o_r.at[h], {"dp": mate})
+
+    def o_arrival(c):
+        return remote(normed.at[c], normed.at[c], o_s.at[s], o_r.at[c], {"dp": mate})
+
+    def work():
+        blocks = lat_all // BLOCK
+        per = length // BLOCK
+
+        @pl.when(is_leader)
+        def _():
+            for b in others():
+                remote(lat.at[b, t], lat.at[b, t], lo_s, lo_r.at[b], {"sp": s}).wait_recv()
+                for k in range(1, n_tp):
+                    lat_plane(b, k, t, tp_peer(k)).start()
+            for b in others():
+                view = ctx.at[b, :, ctx_cols(t)]
+                remote(view, view, cx_s, cx_r.at[b], {"sp": s}).wait_recv()
+                for k in range(1, n_tp):
+                    ctx_plane(b, k, t, tp_peer(k)).start()
+            lat[s, t] = latents[...]
+            mods_arrive()
+            for i, b in enumerate([s] + others()):
+                for k in range(1, n_tp):
+                    lat_plane(b, k, tp_from(k), t).wait_recv()
+                for u in range(n_tp):
+                    put(lat[b, u], 0, b * length + u * rows)
+                lat_hid(b).start()
+                if i == 0:
+                    relay(0, 1)
+                    extras[s] = decay_extra[...]
+                    for c in others():
+                        remote(
+                            extras.at[c], extras.at[c], ex_s, ex_r.at[c], {"sp": s}
+                        ).wait_recv()
+                    extra_mate().start()
+                if i == 2:
+                    relay(1, 1)
+
+        @pl.when(is_follower)
+        def _():
+            relay(0, 1)
+            relay(1, 1)
+            mods_arrive()
+            extra_mate().wait_recv()
+            for b in range(n_sp):
+                lat_hid(b).wait_recv()
+
+        def lows(lo, hi):
+            value = dot_nt(hid[0, lo:hi], decay_down[:, 0:depth])
+            for o in range(1, n_sp):
+                value = value + dot_nt(
+                    hid[o, lo:hi], decay_down[:, o * depth : (o + 1) * depth]
+                )
+            return value.astype(BF16)
+
+        def log_decays(low, z):
+            x = dot(low[:, z * rank : (z + 1) * rank], decay_up[z, :, head_cols(DK)])
+            return log_sigmoid(x + decay_bias[z : z + 1, head_cols(DK)]) / SHARP
+
+        low = lows(0, lat_all)
+        relay(2, 1)
+        decays = [log_decays(low, z) for z in range(2)]
+        group = 2 * length
+        row_id = lax.broadcasted_iota(jnp.int32, (group, group), 0)
+        col_id = lax.broadcasted_iota(jnp.int32, (group, group), 1)
+        same = row_id // BLOCK == col_id // BLOCK
+        inner = [same & (col_id <= row_id), same & (col_id >= row_id)]
+
+        def within_of(z):
+            pieces = []
+            for i in range(lat_all // group):
+                line = jnp.concatenate(
+                    [extras[2 * i + e, z, pl.ds(h, 1), :] for e in range(2)], axis=1
+                )
+                extra = jnp.sum(jnp.where(inner[z], line, 0.0), axis=1, keepdims=True)
+                pieces.append(sums(inner[z], decays[z][i * group : (i + 1) * group]) + extra)
+            return jnp.concatenate(pieces, axis=0)
+
+        within = [within_of(z) for z in range(2)]
+        totals = [
+            [within[0][(b + 1) * BLOCK - 1 : (b + 1) * BLOCK] for b in range(blocks)],
+            [within[1][b * BLOCK : b * BLOCK + 1] for b in range(blocks)],
+        ]
+        none = jnp.zeros_like(totals[0][0])
+
+        def between(z, lo, hi):
+            value = none
+            for b in range(lo, hi):
+                value = value + totals[z][b]
+            return value
+
+        def per_block(f):
+            return jnp.concatenate([f(b) for b in range(blocks)], axis=0)
+
+        def rows_of(x, b):
+            return x[b * BLOCK : (b + 1) * BLOCK]
+
+        def key_span(z, i):
+            if z == 0:
+                return 0, min(-(-(i + 1) * BLOCK // DK) * DK, lat_all)
+            return i * BLOCK // DK * DK, lat_all
+
+        reach = [jnp.exp(within[z]) for z in range(2)]
+        lifted_by = [
+            jnp.exp(per_block(lambda b: rows_of(within[0], b) + between(0, 0, b))),
+            jnp.exp(per_block(lambda b: rows_of(within[1], b) + between(1, b + 1, blocks))),
+        ]
+
+        @pl.when(is_leader)
+        def _():
+            for i in range(ctx_rows // piece):
+                put(
+                    context[i * piece : (i + 1) * piece],
+                    1,
+                    lat_all + s * ctx_rows + i * piece,
+                )
+            ctx_hid(s).start()
+            for b in others():
+                for k in range(1, n_tp):
+                    ctx_plane(b, k, tp_from(k), t).wait_recv()
+                for i in range(ctx_rows // piece):
+                    put(
+                        ctx[b, i * piece : (i + 1) * piece],
+                        1,
+                        lat_all + b * ctx_rows + i * piece,
+                    )
+                ctx_hid(b).start()
+
+        @pl.when(is_follower)
+        def _():
+            for b in range(n_sp):
+                ctx_hid(b).wait_recv()
+
+        low_ctx = lows(lat_all, total)
+        ctx_decays = [log_decays(low_ctx, z) for z in range(2)]
+        ctx_all = total - lat_all
+        crow = lax.broadcasted_iota(jnp.int32, (ctx_all, ctx_all), 0)
+        ccol = lax.broadcasted_iota(jnp.int32, (ctx_all, ctx_all), 1)
+        ctx_weight = [
+            jnp.exp(sums(ccol > crow, ctx_decays[0])),
+            jnp.exp(sums(ccol < crow, ctx_decays[1])),
+        ]
+
+        acc_k[...] = dot(hid[s], wk[s])
+        acc_v[...] = dot(hid[s], wv[s])
+        acc_q[...] = dot(hid[s, 0:lat_all], wq[s])
+        multiply(0, 1, acc_k, total)
+        multiply(1, 1, acc_v, total)
+        multiply(2, 1, acc_q, lat_all)
+        far = range(2, n_sp // 2 + 1)
+        for j in far:
+            relay(0, j)
+            multiply(0, j, acc_k, total)
+        keys = acc_k[...].astype(BF16).astype(F32)
+        ckeys = keys[lat_all:]
+        keys = keys[:lat_all]
+        for z in range(2):
+            close = (keys * jnp.exp(-within[z])).astype(BF16)
+            near = keys * jnp.exp(per_block(lambda b: totals[z][b] - rows_of(within[z], b)))
+            for i in range(blocks):
+                lo, hi = key_span(z, i)
+                for j in range(lo // BLOCK, hi // BLOCK):
+                    if (j > i) if z == 0 else (j < i):
+                        block = jnp.zeros((BLOCK, DK), BF16)
+                    elif i == j:
+                        block = rows_of(close, j)
+                    else:
+                        gap = between(z, min(i, j) + 1, max(i, j))
+                        block = (rows_of(near, j) * jnp.exp(gap)).astype(BF16)
+                    key_rows[z, i, j * BLOCK : (j + 1) * BLOCK] = block
+        for j in far:
+            relay(1, j)
+            multiply(1, j, acc_v, total)
+        values = acc_v[...].astype(BF16)
+        cvals = values[lat_all:]
+        values = values[:lat_all]
+        state = [
+            (CTX_LIFT * dot_tn(cvals, (ckeys * ctx_weight[z]).astype(BF16))).astype(BF16)
+            for z in range(2)
+        ]
+        for j in far:
+            relay(2, j)
+            multiply(2, j, acc_q, lat_all)
+        queries = acc_q[...].astype(BF16).astype(F32)
+        query_dec = [(queries * reach[z]).astype(BF16) for z in range(2)]
+        lifted = [(queries * lifted_by[z]).astype(BF16) for z in range(2)]
+
+        tri_row = lax.broadcasted_iota(jnp.int32, (BLOCK, lat_all), 0)
+        tri_col = lax.broadcasted_iota(jnp.int32, (BLOCK, lat_all), 1)
+
+        def attend(b):
+            lines = []
+            for i in range(b * per, (b + 1) * per):
+                full = []
+                for z in range(2):
+                    lo, hi = key_span(z, i)
+                    score = dot_nt(rows_of(query_dec[z], i), key_rows[z, i, lo:hi])
+                    ids = tri_row[:, lo:hi] + i * BLOCK
+                    cols = tri_col[:, lo:hi]
+                    keep = cols <= ids if z == 0 else cols >= ids
+                    score = jnp.where(keep, score, 0.0)
+                    pads = [jnp.zeros((BLOCK, lo), F32), score, jnp.zeros((BLOCK, lat_all - hi), F32)]
+                    full.append(jnp.concatenate([p for p in pads if p.shape[1]], axis=1))
+                lines.append((full[0] + full[1]).astype(BF16))
+            mixed = dot(jnp.concatenate(lines, axis=0), values)
+            for z in range(2):
+                mixed = mixed + dot_nt(lifted[z][b * length : (b + 1) * length], state[z])
+            by = lax.rsqrt(jnp.mean(mixed * mixed, axis=-1, keepdims=True) + EPS)
+            return (mixed * by * head_gain[...]).astype(BF16)
+
+        for w in range(2):
+
+            @pl.when(side == w)
+            def _():
+                here = first_plane + w
+                order = sorted(range(n_sp), key=lambda b: -abs(b - here))
+                for b in order:
+                    if b != here:
+                        o_out[b] = attend(b)
+                        o_copy(b).start()
+                        continue
+                    result = attend(b)
+
+                    @pl.when(is_leader)
+                    def _():
+                        normed[h] = result
+
+                    @pl.when(is_follower)
+                    def _():
+                        o_out[b] = result
+                        o_mate().start()
+
+    pl.when(is_worker)(work)
+
+    @pl.when(jnp.logical_not(is_worker))
+    def _():
+        mods_arrive()
+
+    @pl.when(is_leader)
+    def _():
+        o_arrival(1 - h).wait_recv()
+
+    @pl.when(is_sender)
+    def _():
+        for c in range(heads):
+            o_arrival(c).wait_recv()
+
+    gate = mod_part(2)[0:1]
+    out_load.wait()
+    chunks = rs_s.shape[1]
+    span = width // chunks
+    rs_copies = []
+    for c in range(chunks):
+        cols = slice(c * span, (c + 1) * span)
+        product = dot(normed[0], wo[0:dv, cols])
+        for g in range(1, heads):
+            product = product + dot(normed[g], wo[g * dv : (g + 1) * dv, cols])
+        product = product.astype(BF16)
+        for i in range(n_tp):
+            part[i, :, cols] = product[i * rows : (i + 1) * rows]
+        for k in range(1, n_tp):
+            to = tp_peer(k)
+            copy = remote(
+                part.at[to, :, pl.ds(c * span, span)],
+                rs.at[k, :, pl.ds(c * span, span)],
+                rs_s.at[k, c],
+                rs_r.at[k, c],
+                {"tp": to},
+            )
+            copy.start()
+            rs_copies.append(copy)
+    for c in range(chunks):
+        cols = slice(c * span, (c + 1) * span)
+        summed = part[t, :, cols].astype(F32)
+        for k in range(1, n_tp):
+            rs_copies[c * (n_tp - 1) + k - 1].wait_recv()
+            summed = summed + rs[k, :, cols].astype(F32)
+        projected = summed.astype(BF16).astype(F32)
+        out[:, cols] = (latents[:, cols].astype(F32) + gate[:, cols] * projected).astype(BF16)
+
+    for copy in rs_copies:
+        copy.wait_send()
+    for k in range(1, n_tp):
+        mod_tp(k, t, tp_peer(k)).wait_send()
+    for k in range(1, n_sp):
+        mod_sp(k, s, sp_peer(k)).wait_send()
+
+    @pl.when(is_sender)
+    def _():
+        lat_in(s, target).wait_send()
+        extra_in(s, target).wait_send()
+        ctx_in(s, target).wait_send()
+
+    @pl.when(is_leader)
+    def _():
+        extra_mate().wait_send()
+        for k in range(1, n_tp):
+            lat_own(k).wait_send()
+            for b in others():
+                lat_plane(b, k, t, tp_peer(k)).wait_send()
+                ctx_plane(b, k, t, tp_peer(k)).wait_send()
+        for b in range(n_sp):
+            lat_hid(b).wait_send()
+            ctx_hid(b).wait_send()
+
+    @pl.when(is_follower)
+    def _():
+        o_mate().wait_send()
+
+    @pl.when(is_worker)
+    def _():
+        for b in others():
+            o_copy(b).wait_send()
+
+    for m in range(3):
+        for r in range(2):
+
+            @pl.when(onward(r))
+            def _():
+                ring_copy(m, r, 0).wait_send()
+
+            for j in range(1, n_sp // 2 + 1):
+
+                @pl.when(jnp.logical_and(exists(r, j), onward(r)))
+                def _():
+                    ring_copy(m, r, j).wait_send()
+
+
+def per_device(n_sp, n_tp, *args):
+    (latents, sv, context, cv, gain, modulator, wq, wk, wv, down, up, bias, extra, hg, wo) = args
+    heads = bias.shape[1] // DK
+    if n_sp != 4 or heads != 2:
+        return chain_per_device(n_sp, n_tp, *args)
+    rows, width = latents.shape
+    ctx_rows = context.shape[0]
+    n_dev = n_sp * n_tp
+    length = rows * n_tp
+    lat_all = n_sp * length
+    total = n_sp * (length + ctx_rows)
+    depth = wq.shape[0]
+    dv = hg.shape[0]
+    chunks = 4
+    vmem = pl.BlockSpec(memory_space=pltpu.VMEM)
+    hbm = pl.BlockSpec(memory_space=pl.ANY)
+    dma = pltpu.SemaphoreType.DMA
+    scratch = [
+        pltpu.VMEM(latents.shape, BF16),
+        pltpu.VMEM(sv.shape, F32),
+        pltpu.VMEM(context.shape, BF16),
+        pltpu.VMEM(cv.shape, F32),
+        pltpu.VMEM((1, width), F32),
+        pltpu.VMEM(down.shape[::-1], BF16),
+        pltpu.VMEM(up.shape, BF16),
+        pltpu.VMEM(bias.shape, F32),
+        pltpu.VMEM((2, heads, length), F32),
+        pltpu.VMEM((1, dv), F32),
+        pltpu.VMEM(modulator.shape, BF16),
+        pltpu.VMEM((n_dev, 2, modulator.shape[1]), F32),
+        pltpu.VMEM((n_sp, n_tp, rows, width), BF16),
+        pltpu.VMEM((n_sp, ctx_rows, width), BF16),
+        pltpu.VMEM((n_sp, 2, heads, length), F32),
+        pltpu.VMEM((n_sp, total, depth), BF16),
+        pltpu.VMEM((n_sp, depth, DK), BF16),
+        pltpu.VMEM((n_sp, depth, dv), BF16),
+        pltpu.VMEM((n_sp, depth, DK), BF16),
+        pltpu.VMEM(wo.shape, BF16),
+        pltpu.VMEM((total, DK), F32),
+        pltpu.VMEM((total, dv), F32),
+        pltpu.VMEM((lat_all, DK), F32),
+        pltpu.VMEM((2, lat_all // BLOCK, lat_all, DK), BF16),
+        pltpu.VMEM((n_sp, length, dv), BF16),
+        pltpu.VMEM((heads, length, dv), BF16),
+        pltpu.VMEM((n_tp, rows, width), BF16),
+        pltpu.VMEM((n_tp, rows, width), BF16),
+        dma((18,)),
+        dma((n_tp,)),
+        dma((n_tp,)),
+        dma((n_sp,)),
+        dma((n_sp,)),
+        dma,
+        dma((n_sp,)),
+        dma,
+        dma((n_sp,)),
+        dma,
+        dma((n_sp,)),
+        dma,
+        dma,
+        dma((n_sp, n_tp)),
+        dma((n_sp, n_tp)),
+        dma((n_sp, n_tp)),
+        dma((n_sp, n_tp)),
+        dma((2 * n_sp,)),
+        dma((2 * n_sp,)),
+        dma((3, 2, n_sp)),
+        dma((3, 2, n_sp)),
+        dma((n_sp,)),
+        dma((heads,)),
+        dma((n_tp, chunks)),
+        dma((n_tp, chunks)),
+    ]
+    return pl.pallas_call(
         functools.partial(kernel, n_sp, n_tp),
         out_shape=jax.ShapeDtypeStruct(latents.shape, BF16),
         in_specs=[hbm] * 15,

time: 59.5 us -> 51.8 us (0.87)
  Pallas kernels: 57.8 us -> 50.1 us
    pallas_call x1, Pallas kernels: 57.8 us -> 50.1 us  [per_device(): pl.pallas_call(functools.partial(kernel, n_sp, n_tp), out_shape=jax.Shape...]
where the time goes in v2:
time: 51.8 us; the launch traced here: 51.6 us
  Pallas kernels  50.1 us (97%)
  local copies, waits for them, and re-layouts  1.57 us (3%)
    pallas_call x1, Pallas kernels, per_device(): pl.pallas_call(functools.partial(kernel, n_sp, n_tp), out_shape=jax.Shape...  50.1 us
    unnamed x1, local copies, waits for them, and re-layouts  1.57 us

profile of v2, /device:TPU:0, one launch (start us, length us, event | category | flops | bytes accessed | tf_op | source)
XLA Modules:
  0.0 51.6 jit_solution(15772563837992703311)
XLA Ops:
  0.0 50.1 %shard_map.145 = bf16[32,2048]{1,0:T(8,128)(2,1)} custom-call(bf16[32,2048]{1,0:T(8,128)(2,1)} %latents_in.1, f32[1,2048]{1,0:T(1,128)} %sample_vector_in.1, bf16[64,2048]{1,0:T(8,128)(2,1)} %context_in.1, f32[1,2048]{1,0:T(1,128)} %context_vector_in.1, f32[1,2048]{1,0:T(1,128)} %bitcast.5, bf16[2048,384]{1,0:T(8,128)(2,1)} %modulator.1, ...), custom_call_target="tpu_custom_call" | custom-call | tf_op jit(solution)/shard_map/pallas_call | solution.py:1627
  50.1 1.6 %copy.17 = bf16[32,2048]{1,0:T(8,128)(2,1)} copy(bf16[32,2048]{1,0:T(8,128)(2,1)} %shard_map.145) | data formatting | bytes 262144

commit v3 on v2

--- a/solution.py
+++ b/solution.py
@@ -975,6 +975,7 @@
     o_r,
     rs_s,
     rs_r,
+    vouch,
 ):
     s = lax.axis_index("sp")
     t = lax.axis_index("tp")
@@ -1035,11 +1036,26 @@
     mod_load = pltpu.make_async_copy(modulator, mod_w, loc_sem.at[0])
     out_load = pltpu.make_async_copy(out_weight, wo, loc_sem.at[4])
     barrier = pltpu.get_barrier_semaphore()
-    for k in range(1, n_tp):
-        pl.semaphore_signal(barrier, inc=1, device_id={"tp": tp_peer(k)}, device_id_type=MESH)
-    for k in range(1, n_sp):
-        pl.semaphore_signal(barrier, inc=1, device_id={"sp": sp_peer(k)}, device_id_type=MESH)
-    pl.semaphore_signal(barrier, inc=1, device_id={"dp": mate}, device_id_type=MESH)
+
+    def signal(semaphore, device):
+        pl.semaphore_signal(semaphore, inc=1, device_id=device, device_id_type=MESH)
+
+    above = s + 1 < n_sp
+    below = s > 0
+    twist = t + 1 - 2 * lax.rem(t, 2)
+    cross = lax.rem(t + 2, n_tp)
+    signal(barrier, {"tp": twist})
+    signal(barrier, {"tp": cross})
+    signal(barrier, {"dp": mate})
+
+    @pl.when(above)
+    def _():
+        signal(barrier, {"sp": s + 1})
+
+    @pl.when(below)
+    def _():
+        signal(barrier, {"sp": s - 1})
+
     small = [
         pltpu.make_async_copy(source, where, loc_sem.at[8 + i])
         for i, (source, where) in enumerate(
@@ -1061,7 +1077,28 @@
         copy.start()
     for copy in small[2:5] + own_weight:
         copy.wait()
-    pl.semaphore_wait(barrier, n_tp + n_sp - 1)
+    pl.semaphore_wait(barrier, 3 + jnp.where(above, 1, 0) + jnp.where(below, 1, 0))
+    signal(vouch.at[n_sp], {"tp": twist})
+
+    def pass_word(step):
+        @pl.when(jnp.logical_and(below, s + step < n_sp))
+        def _():
+            signal(vouch.at[step], {"sp": s - 1})
+
+        @pl.when(jnp.logical_and(above, s - step >= 0))
+        def _():
+            signal(vouch.at[0 if step == 1 else n_sp - 1], {"sp": s + 1})
+
+    def hear_word(step):
+        @pl.when(s + step + 1 < n_sp)
+        def _():
+            pl.semaphore_wait(vouch.at[step], 1)
+
+        @pl.when(s - step - 1 >= 0)
+        def _():
+            pl.semaphore_wait(vouch.at[0 if step == 1 else n_sp - 1], 1)
+
+    pass_word(1)
 
     def onward(r):
         return s + 1 <= last_plane if r == 0 else s - 1 >= first_plane
@@ -1151,23 +1188,46 @@
         steps = sorted(range(-first_plane, n_sp // 2 + 1), key=abs)
         return [s + towards * step for step in steps if step]
 
-    @pl.when(is_sender)
-    def _():
+    adjacent = jnp.logical_or(s == target + 1, s == target - 1)
+
+    def send_rows():
         lat_in(s, target).start()
         extra_in(s, target).start()
         ctx_in(s, target).start()
 
-    @pl.when(is_leader)
-    def _():
-        for k in range(1, n_tp):
-            lat_own(k).start()
-
-    for m in range(3):
+    def send_weight(m):
         for r in range(2):
 
             @pl.when(onward(r))
             def _():
                 ring_copy(m, r, 0).start()
+
+    pl.when(adjacent)(send_rows)
+
+    @pl.when(is_leader)
+    def _():
+        for k in (1, 2, 3):
+
+            @pl.when(tp_peer(k) != lax.rem(twist + 2, n_tp))
+            def _():
+                lat_own(k).start()
+
+    send_weight(0)
+    hear_word(1)
+    pass_word(2)
+    pl.semaphore_wait(vouch.at[n_sp], 1)
+    pl.when(jnp.logical_and(is_sender, jnp.logical_not(adjacent)))(send_rows)
+
+    @pl.when(is_leader)
+    def _():
+        for k in (1, 2, 3):
+
+            @pl.when(tp_peer(k) == lax.rem(twist + 2, n_tp))
+            def _():
+                lat_own(k).start()
+
+    send_weight(1)
+    send_weight(2)
 
     small[0].wait()
     small[1].wait()
@@ -1189,6 +1249,7 @@
         mod_tp(k, t, tp_peer(k)).start()
     for k in range(1, n_tp):
         mod_tp(k, tp_from(k), t).wait_recv()
+    hear_word(2)
     for k in range(1, n_sp):
         mod_sp(k, s, sp_peer(k)).start()
     for copy in small[5:]:
@@ -1407,20 +1468,20 @@
         for j in far:
             relay(2, j)
             multiply(2, j, acc_q, lat_all)
-        queries = acc_q[...].astype(BF16).astype(F32)
-        query_dec = [(queries * reach[z]).astype(BF16) for z in range(2)]
-        lifted = [(queries * lifted_by[z]).astype(BF16) for z in range(2)]
-
         tri_row = lax.broadcasted_iota(jnp.int32, (BLOCK, lat_all), 0)
         tri_col = lax.broadcasted_iota(jnp.int32, (BLOCK, lat_all), 1)
 
         def attend(b):
             lines = []
+            part_of = slice(b * length, (b + 1) * length)
+            queries = acc_q[part_of].astype(BF16).astype(F32)
+            query_dec = [(queries * reach[z][part_of]).astype(BF16) for z in range(2)]
+            lifted = [(queries * lifted_by[z][part_of]).astype(BF16) for z in range(2)]
             for i in range(b * per, (b + 1) * per):
                 full = []
                 for z in range(2):
                     lo, hi = key_span(z, i)
-                    score = dot_nt(rows_of(query_dec[z], i), key_rows[z, i, lo:hi])
+                    score = dot_nt(rows_of(query_dec[z], i - b * per), key_rows[z, i, lo:hi])
                     ids = tri_row[:, lo:hi] + i * BLOCK
                     cols = tri_col[:, lo:hi]
                     keep = cols <= ids if z == 0 else cols >= ids
@@ -1430,7 +1491,7 @@
                 lines.append((full[0] + full[1]).astype(BF16))
             mixed = dot(jnp.concatenate(lines, axis=0), values)
             for z in range(2):
-                mixed = mixed + dot_nt(lifted[z][b * length : (b + 1) * length], state[z])
+                mixed = mixed + dot_nt(lifted[z], state[z])
             by = lax.rsqrt(jnp.mean(mixed * mixed, axis=-1, keepdims=True) + EPS)
             return (mixed * by * head_gain[...]).astype(BF16)
 
@@ -1555,7 +1616,7 @@
 def per_device(n_sp, n_tp, *args):
     (latents, sv, context, cv, gain, modulator, wq, wk, wv, down, up, bias, extra, hg, wo) = args
     heads = bias.shape[1] // DK
-    if n_sp != 4 or heads != 2:
+    if n_sp != 4 or n_tp != 4 or heads != 2:
         return chain_per_device(n_sp, n_tp, *args)
     rows, width = latents.shape
     ctx_rows = context.shape[0]
@@ -1623,6 +1684,7 @@
         dma((heads,)),
         dma((n_tp, chunks)),
         dma((n_tp, chunks)),
+        pltpu.SemaphoreType.REGULAR((n_sp + n_tp,)),
     ]
     return pl.pallas_call(
         functools.partial(kernel, n_sp, n_tp),

time: 51.8 us -> 51 us (0.985)
  Pallas kernels: 50.1 us -> 49.3 us
    pallas_call x1, Pallas kernels: 50.1 us -> 49.3 us  [per_device(): pl.pallas_call(functools.partial(kernel, n_sp, n_tp), out_shape=jax.Shape...]
where the time goes in v3:
time: 51 us; the launch traced here: 50.9 us
  Pallas kernels  49.3 us (97%)
  local copies, waits for them, and re-layouts  1.57 us (3%)
    pallas_call x1, Pallas kernels, per_device(): pl.pallas_call(functools.partial(kernel, n_sp, n_tp), out_shape=jax.Shape...  49.3 us
    unnamed x1, local copies, waits for them, and re-layouts  1.57 us

profile of v3, /device:TPU:0, one launch (start us, length us, event | category | flops | bytes accessed | tf_op | source)
XLA Modules:
  0.0 50.9 jit_solution(368374214452256786)
XLA Ops:
  0.0 49.3 %shard_map.145 = bf16[32,2048]{1,0:T(8,128)(2,1)} custom-call(bf16[32,2048]{1,0:T(8,128)(2,1)} %latents_in.1, f32[1,2048]{1,0:T(1,128)} %sample_vector_in.1, bf16[64,2048]{1,0:T(8,128)(2,1)} %context_in.1, f32[1,2048]{1,0:T(1,128)} %context_vector_in.1, f32[1,2048]{1,0:T(1,128)} %bitcast.5, bf16[2048,384]{1,0:T(8,128)(2,1)} %modulator.1, ...), custom_call_target="tpu_custom_call" | custom-call | tf_op jit(solution)/shard_map/pallas_call | solution.py:1689
  49.3 1.6 %copy.17 = bf16[32,2048]{1,0:T(8,128)(2,1)} copy(bf16[32,2048]{1,0:T(8,128)(2,1)} %shard_map.145) | data formatting | bytes 262144

commit v4 on v3

--- a/solution.py
+++ b/solution.py
@@ -948,6 +948,9 @@
     key_rows,
     o_out,
     normed,
+    duo,
+    wo_twist,
+    kept,
     part,
     rs,
     loc_sem,
@@ -973,6 +976,10 @@
     w_r,
     o_s,
     o_r,
+    wx_s,
+    wx_r,
+    wm_s,
+    wm_r,
     rs_s,
     rs_r,
     vouch,
@@ -1277,17 +1284,49 @@
         for o in range(n_sp):
             hid[o, pl.ds(at, count)] = x[:, o * depth : (o + 1) * depth]
 
-    def o_copy(b):
-        lead = jnp.where(side == h, d, mate)
-        return remote(
-            o_out.at[b], normed.at[h], o_s.at[b], o_r.at[h], {"sp": b, "dp": lead}
-        )
+    lead = jnp.where(side == h, d, mate)
+    parity = lax.rem(t, 2)
+    two = n_tp // 2
+
+    def inside(b):
+        return first_plane <= b <= last_plane
+
+    def o_copies(b):
+        if inside(b):
+            to = {"sp": b, "dp": lead}
+            return [remote(o_out.at[b], normed.at[h], o_s.at[b, 0], o_r.at[0, h], to)]
+        return [
+            remote(
+                o_out.at[b, pl.ds(two * rank_of, two)],
+                duo.at[group, h],
+                o_s.at[b, group],
+                o_r.at[group, h],
+                {"sp": b, "tp": to, "dp": lead},
+            )
+            for group, (rank_of, to) in enumerate(((parity, t), (1 - parity, twist)))
+        ]
 
     def o_mate():
-        return remote(o_out.at[s], normed.at[h], o_s.at[s], o_r.at[h], {"dp": mate})
+        return remote(o_out.at[s], normed.at[h], o_s.at[s, 0], o_r.at[0, h], {"dp": mate})
 
     def o_arrival(c):
-        return remote(normed.at[c], normed.at[c], o_s.at[s], o_r.at[c], {"dp": mate})
+        return remote(normed.at[c], normed.at[c], o_s.at[s, 0], o_r.at[0, c], {"dp": mate})
+
+    def duo_arrival(group, c):
+        view = duo.at[group, c]
+        return remote(view, view, o_s.at[s, 0], o_r.at[group, c], {"dp": mate})
+
+    half_rows = wo.shape[0] // 2
+
+    def wo_half(where, side_of):
+        return where.at[pl.ds(pl.multiple_of(side_of * half_rows, half_rows), half_rows)]
+
+    def wo_cross():
+        return remote(wo_half(wo, h), wo_half(wo_twist, h), wx_s, wx_r, {"tp": twist})
+
+    def wo_mate(side_of):
+        view = wo_half(wo_twist, side_of)
+        return remote(view, view, wm_s, wm_r, {"dp": mate})
 
     def work():
         blocks = lat_all // BLOCK
@@ -1500,73 +1539,123 @@
             @pl.when(side == w)
             def _():
                 here = first_plane + w
-                order = sorted(range(n_sp), key=lambda b: -abs(b - here))
+                near = here - 1 + 2 * w
+                order = sorted((b for b in range(n_sp) if not inside(b)), key=lambda b: b == near)[:1] + [here + 1 - 2 * w, near, here]
+
+                def store(b, value):
+                    for u in range(n_tp):
+                        at = u if inside(b) else u % 2 * two + u // 2
+                        o_out[b, at] = value[u * rows : (u + 1) * rows]
+
                 for b in order:
+                    result = attend(b)
                     if b != here:
-                        o_out[b] = attend(b)
-                        o_copy(b).start()
+                        store(b, result)
+                        for copy in o_copies(b):
+                            copy.start()
                         continue
-                    result = attend(b)
 
                     @pl.when(is_leader)
                     def _():
-                        normed[h] = result
+                        for u in range(n_tp):
+                            normed[h, u] = result[u * rows : (u + 1) * rows]
 
                     @pl.when(is_follower)
                     def _():
-                        o_out[b] = result
+                        store(b, result)
                         o_mate().start()
 
     pl.when(is_worker)(work)
 
-    @pl.when(jnp.logical_not(is_worker))
+    is_outer = jnp.logical_not(is_worker)
+
+    @pl.when(is_outer)
     def _():
+        out_load.wait()
+        wo_cross().start()
         mods_arrive()
+        wo_cross().wait_recv()
+        wo_mate(h).start()
+        wo_mate(1 - h).wait_recv()
+        for group in range(2):
+            for c in range(heads):
+                duo_arrival(group, c).wait_recv()
 
     @pl.when(is_leader)
     def _():
         o_arrival(1 - h).wait_recv()
 
-    @pl.when(is_sender)
+    @pl.when(is_follower)
     def _():
         for c in range(heads):
             o_arrival(c).wait_recv()
 
-    gate = mod_part(2)[0:1]
-    out_load.wait()
     chunks = rs_s.shape[1]
     span = width // chunks
-    rs_copies = []
-    for c in range(chunks):
-        cols = slice(c * span, (c + 1) * span)
-        product = dot(normed[0], wo[0:dv, cols])
-        for g in range(1, heads):
-            product = product + dot(normed[g], wo[g * dv : (g + 1) * dv, cols])
-        product = product.astype(BF16)
-        for i in range(n_tp):
-            part[i, :, cols] = product[i * rows : (i + 1) * rows]
-        for k in range(1, n_tp):
-            to = tp_peer(k)
-            copy = remote(
-                part.at[to, :, pl.ds(c * span, span)],
-                rs.at[k, :, pl.ds(c * span, span)],
-                rs_s.at[k, c],
-                rs_r.at[k, c],
-                {"tp": to},
-            )
-            copy.start()
-            rs_copies.append(copy)
-    for c in range(chunks):
-        cols = slice(c * span, (c + 1) * span)
-        summed = part[t, :, cols].astype(F32)
-        for k in range(1, n_tp):
-            rs_copies[c * (n_tp - 1) + k - 1].wait_recv()
-            summed = summed + rs[k, :, cols].astype(F32)
+
+    def rs_copy(index, k, c, to):
+        return remote(
+            part.at[index, :, pl.ds(c * span, span)],
+            rs.at[k, :, pl.ds(c * span, span)],
+            rs_s.at[k, c],
+            rs_r.at[k, c],
+            {"tp": to},
+        )
+
+    def write_out(cols, summed):
+        gate = jnp.concatenate([mods[j] for j in range(n_dev)], axis=1)[0:1, 2 * width :]
         projected = summed.astype(BF16).astype(F32)
         out[:, cols] = (latents[:, cols].astype(F32) + gate[:, cols] * projected).astype(BF16)
 
-    for copy in rs_copies:
-        copy.wait_send()
+    @pl.when(is_worker)
+    def _():
+        out_load.wait()
+        for c in range(chunks):
+            cols = slice(c * span, (c + 1) * span)
+            product = 0.0
+            for g in range(heads):
+                product = product + dot(
+                    normed[g].reshape(length, dv), wo[g * dv : (g + 1) * dv, cols]
+                )
+            product = product.astype(BF16)
+            for i in range(n_tp):
+                part[i, :, cols] = product[i * rows : (i + 1) * rows]
+            for k in range(1, n_tp):
+                rs_copy(tp_peer(k), k, c, tp_peer(k)).start()
+        for c in range(chunks):
+            cols = slice(c * span, (c + 1) * span)
+            summed = part[t, :, cols].astype(F32)
+            for k in range(1, n_tp):
+                rs_copy(tp_peer(k), k, c, tp_peer(k)).wait_recv()
+                summed = summed + rs[k, :, cols].astype(F32)
+            write_out(cols, summed)
+        for c in range(chunks):
+            for k in range(1, n_tp):
+                rs_copy(tp_peer(k), k, c, tp_peer(k)).wait_send()
+
+    @pl.when(is_outer)
+    def _():
+        for c in range(chunks):
+            cols = slice(c * span, (c + 1) * span)
+            product = 0.0
+            for group, matrix in enumerate((wo, wo_twist)):
+                for g in range(heads):
+                    product = product + dot(
+                        duo[group, g].reshape(two * rows, dv), matrix[g * dv : (g + 1) * dv, cols]
+                    )
+            low_half = t < two
+            kept[:, cols] = jnp.where(low_half, product[:rows], product[rows:])
+            part[0, :, cols] = jnp.where(low_half, product[rows:], product[:rows]).astype(BF16)
+            rs_copy(0, 1, c, cross).start()
+        for c in range(chunks):
+            cols = slice(c * span, (c + 1) * span)
+            rs_copy(0, 1, c, cross).wait_recv()
+            write_out(cols, kept[:, cols] + rs[1, :, cols].astype(F32))
+        for c in range(chunks):
+            rs_copy(0, 1, c, cross).wait_send()
+        wo_cross().wait_send()
+        wo_mate(h).wait_send()
+
     for k in range(1, n_tp):
         mod_tp(k, t, tp_peer(k)).wait_send()
     for k in range(1, n_sp):
@@ -1594,10 +1683,14 @@
     def _():
         o_mate().wait_send()
 
-    @pl.when(is_worker)
-    def _():
-        for b in others():
-            o_copy(b).wait_send()
+    for w in range(2):
+
+        @pl.when(side == w)
+        def _():
+            for b in range(n_sp):
+                if b != first_plane + w:
+                    for copy in o_copies(b):
+                        copy.wait_send()
 
     for m in range(3):
         for r in range(2):
@@ -1655,8 +1748,11 @@
         pltpu.VMEM((total, dv), F32),
         pltpu.VMEM((lat_all, DK), F32),
         pltpu.VMEM((2, lat_all // BLOCK, lat_all, DK), BF16),
-        pltpu.VMEM((n_sp, length, dv), BF16),
-        pltpu.VMEM((heads, length, dv), BF16),
+        pltpu.VMEM((n_sp, n_tp, rows, dv), BF16),
+        pltpu.VMEM((heads, n_tp, rows, dv), BF16),
+        pltpu.VMEM((2, heads, n_tp // 2, rows, dv), BF16),
+        pltpu.VMEM(wo.shape, BF16),
+        pltpu.VMEM((rows, width), F32),
         pltpu.VMEM((n_tp, rows, width), BF16),
         pltpu.VMEM((n_tp, rows, width), BF16),
         dma((18,)),
@@ -1680,8 +1776,12 @@
         dma((2 * n_sp,)),
         dma((3, 2, n_sp)),
         dma((3, 2, n_sp)),
-        dma((n_sp,)),
-        dma((heads,)),
+        dma((n_sp, 2)),
+        dma((2, heads)),
+        dma,
+        dma,
+        dma,
+        dma,
         dma((n_tp, chunks)),
         dma((n_tp, chunks)),
         pltpu.SemaphoreType.REGULAR((n_sp + n_tp,)),

time: 51 us -> 49.3 us (0.967)
  Pallas kernels: 49.3 us -> 47.4 us
    pallas_call x1, Pallas kernels: 49.3 us -> 47.4 us  [per_device(): pl.pallas_call(functools.partial(kernel, n_sp, n_tp), out_shape=jax.Shape...]
where the time goes in v4:
time: 49.3 us; the launch traced here: 49 us
  Pallas kernels  47.4 us (96%)
  local copies, waits for them, and re-layouts  1.57 us (3%)
    pallas_call x1, Pallas kernels, per_device(): pl.pallas_call(functools.partial(kernel, n_sp, n_tp), out_shape=jax.Shape...  47.4 us
    unnamed x1, local copies, waits for them, and re-layouts  1.57 us

profile of v4, /device:TPU:0, one launch (start us, length us, event | category | flops | bytes accessed | tf_op | source)
XLA Modules:
  0.0 49.0 jit_solution(14329414529626985977)
XLA Ops:
  0.0 47.4 %shard_map.145 = bf16[32,2048]{1,0:T(8,128)(2,1)} custom-call(bf16[32,2048]{1,0:T(8,128)(2,1)} %latents_in.1, f32[1,2048]{1,0:T(1,128)} %sample_vector_in.1, bf16[64,2048]{1,0:T(8,128)(2,1)} %context_in.1, f32[1,2048]{1,0:T(1,128)} %context_vector_in.1, f32[1,2048]{1,0:T(1,128)} %bitcast.5, bf16[2048,384]{1,0:T(8,128)(2,1)} %modulator.1, ...), custom_call_target="tpu_custom_call" | custom-call | tf_op jit(solution)/shard_map/pallas_call | solution.py:1789
  47.4 1.6 %copy.17 = bf16[32,2048]{1,0:T(8,128)(2,1)} copy(bf16[32,2048]{1,0:T(8,128)(2,1)} %shard_map.145) | data formatting | bytes 262144

commit v5 on v4

--- a/solution.py
+++ b/solution.py
@@ -1221,7 +1221,6 @@
 
     send_weight(0)
     hear_word(1)
-    pass_word(2)
     pl.semaphore_wait(vouch.at[n_sp], 1)
     pl.when(jnp.logical_and(is_sender, jnp.logical_not(adjacent)))(send_rows)
 
@@ -1250,15 +1249,21 @@
 
     def mod_sp(k, owner, to):
         view = mods.at[pl.ds(owner * n_tp, n_tp)]
-        return remote(view, view, ms_s.at[k], ms_r.at[k], {"sp": to})
+        return remote(view, view, ms_s.at[k], ms_r.at[owner], {"sp": to})
+
+    low_side = s <= first_plane
+    partner = s + 1 - 2 * lax.rem(s, 2)
+    over = jnp.where(low_side, last_plane, first_plane)
+    beyond = jnp.where(low_side, last_plane, 0)
+    mod_direct = [mod_sp(0, s, partner), mod_sp(1, s, over)]
+    mod_passed = [mod_sp(2 + i, beyond + i, partner) for i in range(2)]
 
     for k in range(1, n_tp):
         mod_tp(k, t, tp_peer(k)).start()
     for k in range(1, n_tp):
         mod_tp(k, tp_from(k), t).wait_recv()
-    hear_word(2)
-    for k in range(1, n_sp):
-        mod_sp(k, s, sp_peer(k)).start()
+    for copy in mod_direct:
+        copy.start()
     for copy in small[5:]:
         copy.wait()
 
@@ -1270,6 +1275,11 @@
     def mods_arrive():
         for k in range(1, n_sp):
             mod_sp(k, sp_from(k), s).wait_recv()
+
+        @pl.when(is_worker)
+        def _():
+            for copy in mod_passed:
+                copy.start()
 
     piece = min(32, ctx_rows)
 
@@ -1658,8 +1668,13 @@
 
     for k in range(1, n_tp):
         mod_tp(k, t, tp_peer(k)).wait_send()
-    for k in range(1, n_sp):
-        mod_sp(k, s, sp_peer(k)).wait_send()
+    for copy in mod_direct:
+        copy.wait_send()
+
+    @pl.when(is_worker)
+    def _():
+        for copy in mod_passed:
+            copy.wait_send()
 
     @pl.when(is_sender)
     def _():
@@ -1719,7 +1734,7 @@
     total = n_sp * (length + ctx_rows)
     depth = wq.shape[0]
     dv = hg.shape[0]
-    chunks = 4
+    chunks = 2
     vmem = pl.BlockSpec(memory_space=pltpu.VMEM)
     hbm = pl.BlockSpec(memory_space=pl.ANY)
     dma = pltpu.SemaphoreType.DMA

time: 49.3 us -> 49.1 us (level)
  no operation moved by 1% of the time
where the time goes in v5:
time: 49.1 us; the launch traced here: 48.9 us
  Pallas kernels  47.3 us (96%)
  local copies, waits for them, and re-layouts  1.57 us (3%)
    pallas_call x1, Pallas kernels, per_device(): pl.pallas_call(functools.partial(kernel, n_sp, n_tp), out_shape=jax.Shape...  47.3 us
    unnamed x1, local copies, waits for them, and re-layouts  1.57 us

profile of v5, /device:TPU:0, one launch (start us, length us, event | category | flops | bytes accessed | tf_op | source)
XLA Modules:
  0.0 48.9 jit_solution(2694096424183307786)
XLA Ops:
  0.0 47.3 %shard_map.145 = bf16[32,2048]{1,0:T(8,128)(2,1)} custom-call(bf16[32,2048]{1,0:T(8,128)(2,1)} %latents_in.1, f32[1,2048]{1,0:T(1,128)} %sample_vector_in.1, bf16[64,2048]{1,0:T(8,128)(2,1)} %context_in.1, f32[1,2048]{1,0:T(1,128)} %context_vector_in.1, f32[1,2048]{1,0:T(1,128)} %bitcast.5, bf16[2048,384]{1,0:T(8,128)(2,1)} %modulator.1, ...), custom_call_target="tpu_custom_call" | custom-call | tf_op jit(solution)/shard_map/pallas_call | solution.py:1804
  47.3 1.6 %copy.17 = bf16[32,2048]{1,0:T(8,128)(2,1)} copy(bf16[32,2048]{1,0:T(8,128)(2,1)} %shard_map.145) | data formatting | bytes 262144
